TPU v7x, 32 devices: a whole 2x2x4 slice. The times are simulated.
32 devices in a mesh: sp: 8 (over z, y), tp: 4 (over x, core).
Axes of the slice: x: 2, y: 2, z: 4, core: 2. Of those that a mesh axis runs over, the one named last changes fastest.
Arguments:
- tokens: bfloat16 [1024, 2048], P(('sp', 'tp')), may hold values from -64 to 64, as said below
- query_one: bfloat16 [2048, 256], P(None, 'tp'), may hold values from -0.125 to 0.125
- query_two: bfloat16 [2048, 256], P(None, 'tp'), may hold values from -0.125 to 0.125
- key_one: bfloat16 [2048, 256], P(None, 'tp'), may hold values from -0.125 to 0.125
- key_two: bfloat16 [2048, 256], P(None, 'tp'), may hold values from -0.125 to 0.125
- value_weight: bfloat16 [2048, 512], P(None, 'tp'), may hold values from -0.125 to 0.125
- mixing: float32 [4], P('tp'), may hold values from 0.3 to 0.8
- out_weight: bfloat16 [512, 2048], replicated, may hold values from -0.25 to 0.25
- head_gain: float32 [128], replicated, may hold values from 0.1 to 1.9
Outputs:
- attended: bfloat16 [1024, 2048], P(('sp', 'tp'))
Inputs may be any that keep to these rules, and one draw needn't show every extreme that they name: `tokens`: Real-valued activations.
All inputs are finite; a program needn't handle non-finite values.
Results may differ from a plain program's by a relative error of at most 0.012.
The roundings to bfloat16 on the way count: a program that leaves them out, or rounds other values in their place, can miss the bound.
Values may be sent and summed in bfloat16 or wider, within the bound.
No kernel may reach another device: no remote copies, remote signals or barrier semaphores. Data moves between devices by JAX's collectives and lax.ppermute only.
A program may use at most 64 MiB of HBM per device.

v0:
```python
import math

import jax
import jax.numpy as jnp
from jax import lax
from jax.sharding import PartitionSpec as P

HEAD = 64
GRID_W = 64


epsilon = 1e-06
theta_base = 10000.0
floor_value = -1e30


def grid_turn(field, positions):
    quarter = field.shape[-1] // 4
    half = 2 * quarter
    freqs = theta_base ** (-jnp.arange(quarter, dtype=jnp.float32) / quarter)
    row_angle = (positions // GRID_W).astype(jnp.float32)[:, None] * freqs
    col_angle = (positions % GRID_W).astype(jnp.float32)[:, None] * freqs

    def turn(segment, angle):
        cosine = jnp.cos(angle)[:, None, :]
        sine = jnp.sin(angle)[:, None, :]
        first = segment[..., :quarter]
        second = segment[..., quarter:]
        return jnp.concatenate(
            [first * cosine - second * sine, first * sine + second * cosine], axis=-1
        )

    return jnp.concatenate(
        [turn(field[..., :half], row_angle), turn(field[..., half:], col_angle)], axis=-1
    )


def one_map(state, queries, keys, values):
    peak, total, summed = state
    scores = jnp.einsum(
        "qhd,khd->qhk", queries, keys, preferred_element_type=jnp.float32
    ) * HEAD ** (-0.5)
    new_peak = jnp.maximum(peak, jnp.max(scores, axis=-1))
    factor = jnp.exp(peak - new_peak)
    weights = jnp.exp(scores - new_peak[..., None])
    total = total * factor + jnp.sum(weights, axis=-1)
    summed = summed * factor[..., None] + jnp.einsum(
        "qhk,khe->qhe", weights.astype(jnp.bfloat16), values, preferred_element_type=jnp.float32
    )
    return (new_peak, total, summed)


def make_absorb(q_first, q_second, head_local):
    cols = head_local * HEAD

    def absorb(carry, piece, start):
        count = piece.shape[0]
        width = math.gcd(count, 2048)

        def step(index, state):
            block = lax.dynamic_slice_in_dim(piece, index * width, width, 0)
            keys_first = block[:, :cols].reshape(width, head_local, HEAD)
            keys_second = block[:, cols : 2 * cols].reshape(width, head_local, HEAD)
            values = block[:, 2 * cols :].reshape(width, head_local, 2 * HEAD)
            return (
                one_map(state[0], q_first, keys_first, values),
                one_map(state[1], q_second, keys_second, values),
            )

        return lax.fori_loop(0, count // width, step, carry)

    return absorb


def per_device(
    tokens, query_one, query_two, key_one, key_two, value_weight, mixing, out_weight, head_gain
):
    groups = lax.axis_size("tp")
    own_rows = tokens.shape[0]
    row_count = own_rows * groups
    head_cols = query_one.shape[1]
    head_local = head_cols // HEAD
    joined = jnp.concatenate([query_one, query_two, key_one, key_two, value_weight], axis=1)
    projected = jnp.dot(
        lax.all_gather(tokens, "tp", axis=0, tiled=True), joined, preferred_element_type=jnp.float32
    )
    positions = lax.axis_index("sp") * row_count + jnp.arange(row_count, dtype=jnp.int32)

    def heads_of(lower, upper):
        return projected[:, lower:upper].reshape(row_count, head_local, HEAD)

    q_first = grid_turn(heads_of(0, head_cols), positions).astype(jnp.bfloat16)
    q_second = grid_turn(heads_of(head_cols, 2 * head_cols), positions).astype(jnp.bfloat16)
    k_first = grid_turn(heads_of(2 * head_cols, 3 * head_cols), positions).astype(jnp.bfloat16)
    k_second = grid_turn(heads_of(3 * head_cols, 4 * head_cols), positions).astype(jnp.bfloat16)
    values = projected[:, 4 * head_cols :].astype(jnp.bfloat16)
    packed = jnp.concatenate(
        [k_first.reshape(row_count, head_cols), k_second.reshape(row_count, head_cols), values],
        axis=1,
    )
    absorb = make_absorb(q_first, q_second, head_local)
    empty = (
        jnp.full((row_count, head_local), floor_value, jnp.float32),
        jnp.zeros((row_count, head_local), jnp.float32),
        jnp.zeros((row_count, head_local, 2 * HEAD), jnp.float32),
    )
    gathered = lax.all_gather(packed, "sp", axis=0, tiled=True)
    first_map, second_map = absorb((empty, empty), gathered, 0)
    mixed = first_map[2] / first_map[1][..., None] - mixing[None, :, None] * (
        second_map[2] / second_map[1][..., None]
    )
    normed = (
        mixed * lax.rsqrt(jnp.mean(mixed * mixed, axis=-1, keepdims=True) + epsilon) * head_gain
    )
    heads = normed.astype(jnp.bfloat16).reshape(row_count, head_local * 2 * HEAD)
    regrouped = lax.all_to_all(heads, "tp", split_axis=0, concat_axis=1, tiled=True)
    summed = jnp.dot(regrouped, out_weight, preferred_element_type=jnp.float32)
    return summed.astype(jnp.bfloat16)


def solution(mesh):
    in_specs = (
        P(("sp", "tp"), None),
        P(None, "tp"),
        P(None, "tp"),
        P(None, "tp"),
        P(None, "tp"),
        P(None, "tp"),
        P("tp"),
        P(),
        P(),
    )
    out_specs = P(("sp", "tp"), None)
    return jax.shard_map(
        per_device, mesh=mesh, in_specs=in_specs, out_specs=out_specs, check_vma=False
    )
```

profile of v0, /device:TPU:0, one launch (start us, length us, event | category | flops | bytes accessed | tf_op | source)
XLA Modules:
  0.0 59.8 jit_solution(14919113349166023938)
XLA Ops:
  0.0 0.0 copy-start
  0.0 0.0 copy-start.1
  0.0 0.0 copy-start.2
  0.0 1.4 %copy.19 = bf16[2048,64]{1,0:T(8,128)(2,1)S(1)} copy(bf16[2048,64]{0,1:T(8,128)(2,1)} %param.10) | data formatting | bytes 524288 | tf_op args[1]
  1.4 2.0 %copy.20 = bf16[2048,64]{1,0:T(8,128)(2,1)} copy(bf16[2048,64]{0,1:T(8,128)(2,1)} %param.11) | data formatting | bytes 524288 | tf_op args[2]
  3.4 2.0 %copy.21 = bf16[2048,64]{1,0:T(8,128)(2,1)} copy(bf16[2048,64]{0,1:T(8,128)(2,1)} %param.12) | data formatting | bytes 524288 | tf_op args[3]
  5.3 0.0 copy-done.1
  5.3 1.0 %copy.22 = bf16[2048,64]{1,0:T(8,128)(2,1)} copy(bf16[2048,64]{0,1:T(8,128)(2,1)S(1)} %copy-done.1) | data formatting | bytes 524288 | tf_op args[4]
  6.4 0.0 copy-done.2
  6.4 8.6 %all_gather.6 = bf16[128,2048]{1,0:T(8,128)(2,1)S(1)} all-gather(bf16[32,2048]{1,0:T(8,128)(2,1)S(1)} %copy-done.2), channel_id=1, replica_groups=mesh['sp'=8,'tp'=4] {'tp'}, dimensions={0}, use_global_device_ids=true | all-gather | bytes 655360 | tf_op jit(solution)/shard_map/all_gather | solution.py:85
  15.0 4.1 %concatenate.63 = bf16[2048,384]{1,0:T(8,128)(2,1)} concatenate(bf16[2048,64]{1,0:T(8,128)(2,1)S(1)} %copy.19, bf16[2048,64]{1,0:T(8,128)(2,1)} %copy.20, bf16[2048,64]{1,0:T(8,128)(2,1)} %copy.21, bf16[2048,64]{1,0:T(8,128)(2,1)} %copy.22, bf16[2048,128]{1,0:T(8,128)(2,1)} %param.14), dimensions={1} | concatenate | bytes 3145728 | tf_op jit(solution)/shard_map/concatenate | solution.py:83
  19.1 2.0 %convolution_bitcast_fusion = f32[128,384]{0,1:T(8,128)S(1)} fusion(bf16[2048,384]{1,0:T(8,128)(2,1)} %concatenate.63, bf16[128,2048]{1,0:T(8,128)(2,1)S(1)} %all_gather.6), kind=kOutput, calls=%fused_computation.3 | convolution fusion | flops 201326592 | bytes 2293760 | tf_op jit(solution)/shard_map/dot_general | solution.py:84
  21.2 0.1 constant_dynamic-update-slice_fusion.7
  21.3 0.1 constant_dynamic-update-slice_fusion.6
  21.4 0.1 constant_dynamic-update-slice_fusion.5
  21.5 0.1 constant_dynamic-update-slice_fusion.4
  21.7 0.1 constant_dynamic-update-slice_fusion.3
  21.8 0.1 constant_dynamic-update-slice_fusion.2
  21.9 0.1 constant_dynamic-update-slice_fusion.1
  22.1 0.1 constant_dynamic-update-slice_fusion
  22.2 27.5 %all_gather.7 = bf16[1024,256]{0,1:T(8,128)(2,1)S(1)} all-gather(bf16[128,256]{0,1:T(8,128)(2,1)S(1)} %fusion.22), channel_id=1, replica_groups=mesh['sp'=8,'tp'=4] {'sp'}, dimensions={0}, use_global_device_ids=true | all-gather | bytes 589824 | tf_op jit(solution)/shard_map/all_gather | solution.py:107
  49.7 0.2 fusion.108
  49.8 0.0 copy-start.3
  49.8 0.3 fusion.117
  50.2 0.2 fusion.10
  51.0 0.3 fusion.118
  51.4 0.2 fusion.8
  51.5 0.3 fusion.5
  51.8 0.4 multiply_reduce_fusion
  52.2 0.0 copy-done.3
  52.2 0.1 multiply_convert_fusion
  52.3 6.3 %all_to_all.19 = bf16[4,32,128]{2,1,0:T(8,128)(2,1)S(1)} all-to-all(bf16[4,32,128]{2,1,0:T(8,128)(2,1)S(1)} %bitcast.110), channel_id=1, replica_groups=mesh['sp'=8,'tp'=4] {'tp'}, dimensions={0} | all-to-all | bytes 65536 | tf_op jit(solution)/shard_map/all_to_all | solution.py:116
  58.6 0.0 copy-done
  58.6 1.1 %convolution_convert_fusion = bf16[32,2048]{1,0:T(8,128)(2,1)} fusion(bf16[512,2048]{1,0:T(8,128)(2,1)S(1)} %copy-done, bf16[4,32,128]{2,1,0:T(8,128)(2,1)S(1)} %all_to_all.19), kind=kOutput, calls=%fused_computation | convolution fusion | flops 67174400 | bytes 2260992 | tf_op jit(solution)/shard_map/dot_general | solution.py:117
  (9 shorter events, 0.1 us)
Async XLA Ops:
  0.0 58.6 %copy-start = (bf16[512,2048]{1,0:T(8,128)(2,1)S(1)}, bf16[512,2048]{1,0:T(8,128)(2,1)}, u32[]{:S(2)}) copy-start(bf16[512,2048]{1,0:T(8,128)(2,1)} %param.16) | copy-start | bytes 6291460
  0.0 5.3 %copy-start.1 = (bf16[2048,64]{0,1:T(8,128)(2,1)S(1)}, bf16[2048,64]{0,1:T(8,128)(2,1)}, u32[]{:S(2)}) copy-start(bf16[2048,64]{0,1:T(8,128)(2,1)} %param.13) | copy-start | bytes 786436
  0.0 6.4 %copy-start.2 = (bf16[32,2048]{1,0:T(8,128)(2,1)S(1)}, bf16[32,2048]{1,0:T(8,128)(2,1)}, u32[]{:S(2)}) copy-start(bf16[32,2048]{1,0:T(8,128)(2,1)} %param.9) | copy-start | bytes 393220
  49.8 2.4 %copy-start.3 = (f32[128]{0:T(128)S(1)}, f32[128]{0:T(128)}, u32[]{:S(2)}) copy-start(f32[128]{0:T(128)} %param.17) | copy-start | bytes 1540
where the time goes:
time: 60.1 us; the launch traced here: 59.8 us
  blocking collectives  42.4 us (71%)
  local copies, waits for them, and re-layouts  10.5 us (17%)
  matrix products  4.48 us (7%)
  other arithmetic  1.64 us (3%)
  between operations  0.75 us (1%)
    all_gather x1, blocking collectives, per_device(): gathered = lax.all_gather(packed, 'sp', axis=0, tiled=True)  27.5 us
    all_gather x1, blocking collectives, per_device(): lax.all_gather(tokens, 'tp', axis=0, tiled=True)  8.64 us
    unnamed x12, local copies, waits for them, and re-layouts  6.35 us
    all_to_all x1, blocking collectives, per_device(): lax.all_to_all(heads, 'tp', split_axis=0, concat_axis=1, tiled=True)  6.3 us
    concatenate x1, local copies, waits for them, and re-layouts, per_device(): jnp.concatenate([query_one, query_two, key_one, key_two, value_weight], a...  4.1 us
    dot_general x1, matrix products, per_device(): jnp.dot(lax.all_gather(tokens, 'tp', axis=0, tiled=True), joined, preferr...  2.01 us

commit v1 on v0

v1 whole, which is shorter than its diff:
```python
import functools

import jax
import jax.numpy as jnp
import numpy as np
from jax import lax
from jax.experimental import pallas as pl
from jax.experimental.pallas import tpu as pltpu
from jax.sharding import PartitionSpec as P

HEAD = 64
GRID_W = 64
PAIR = 2 * HEAD

epsilon = 1e-06
theta_base = 10000.0
floor_value = -1e30
ring_limit = 16
chunk_rows = 1024
log2_e = 1.4426950408889634
MIB = 1 << 20
stage_grant = 52 * MIB

CONTRACT_LAST = (((1,), (1,)), ((), ()))


def turn_of(start, count):
    quarter = HEAD // 4
    lane = lax.broadcasted_iota(jnp.int32, (1, PAIR), 1)
    index = lane % quarter
    freqs = jnp.zeros((1, PAIR), jnp.float32)
    for j in range(quarter):
        freqs = jnp.where(index == j, theta_base ** (-j / quarter), freqs)
    token = start + lax.broadcasted_iota(jnp.int32, (count, PAIR), 0)
    by_row = (lane & (HEAD // 2)) == 0
    position = jnp.where(by_row, token // GRID_W, token % GRID_W).astype(jnp.float32)
    angle = position * freqs
    sine = jnp.sin(angle)
    return jnp.cos(angle), jnp.where((lane & quarter) == 0, -sine, sine)


def turned(field, cosine, sine):
    lane = lax.broadcasted_iota(jnp.int32, field.shape, 1)
    ahead = pltpu.roll(field, PAIR - HEAD // 4, 1)
    behind = pltpu.roll(field, HEAD // 4, 1)
    partner = jnp.where((lane & (HEAD // 4)) == 0, ahead, behind)
    return (field * cosine + partner * sine).astype(jnp.bfloat16)


def project_block(tokens, start, weight_refs, heads, q_ref, kv_ref, place):
    one_q, two_q, one_k, two_k, upper, lower = weight_refs
    count = tokens.shape[0]
    cosine, sine = turn_of(start, count)
    for head in range(heads):
        rows = slice(head * HEAD, (head + 1) * HEAD)

        def pair(first_w, second_w):
            return jnp.concatenate(
                [
                    lax.dot_general(
                        tokens, w[rows, :], CONTRACT_LAST, preferred_element_type=jnp.float32
                    )
                    for w in (first_w, second_w)
                ],
                axis=1,
            )

        columns = slice(head * PAIR, (head + 1) * PAIR)
        base = head * 2 * PAIR
        q_ref[place, columns] = turned(pair(one_q, two_q), cosine, sine)
        kv_ref[place, base : base + PAIR] = turned(pair(one_k, two_k), cosine, sine)
        half = upper.shape[0]
        values = jnp.dot(
            tokens[:, :half], upper[:, columns], preferred_element_type=jnp.float32
        ) + jnp.dot(tokens[:, half:], lower[:, columns], preferred_element_type=jnp.float32)
        kv_ref[place, base + PAIR : base + 2 * PAIR] = values.astype(jnp.bfloat16)


def start_of(step, count, groups):
    return (lax.axis_index("sp") * groups + (lax.axis_index("tp") ^ step)) * count


def stage_kernel(count, *refs):
    sources, held, sems = refs[:count], refs[count:-1], refs[-1]
    half = sources[-1].shape[0] // 2
    sources = [*sources[:-1], sources[-1].at[pl.ds(0, half)], sources[-1].at[pl.ds(half, half)]]
    copies = [pltpu.make_async_copy(a, b, sems.at[i]) for i, (a, b) in enumerate(zip(sources, held))]
    for copy in copies:
        copy.start()
    for copy in copies:
        copy.wait()


def shapes_of(rows, heads):
    return [
        jax.ShapeDtypeStruct((rows, heads * PAIR), jnp.bfloat16),
        jax.ShapeDtypeStruct((rows, heads * 2 * PAIR), jnp.bfloat16),
    ]


def project_cost(rows, depth, heads):
    return pl.CostEstimate(
        flops=2 * rows * depth * heads * 3 * PAIR, bytes_accessed=0, transcendentals=0
    )


def stage(arrays):
    size = sum(a.size * 2 for a in arrays)
    rows, columns = arrays[-1].shape
    shapes = [a.shape for a in arrays[:-1]] + [(rows // 2, columns)] * 2
    return pl.pallas_call(
        functools.partial(stage_kernel, len(arrays)),
        out_shape=[jax.ShapeDtypeStruct(shape, arrays[0].dtype) for shape in shapes],
        in_specs=[pl.BlockSpec(memory_space=pltpu.HBM)] * len(arrays),
        scratch_shapes=[pltpu.SemaphoreType.DMA((len(shapes),))],
        cost_estimate=pl.CostEstimate(flops=size * 256, bytes_accessed=size, transcendentals=0),
        compiler_params=pltpu.CompilerParams(vmem_limit_bytes=stage_grant),
        name="stage",
    )(*arrays)


def project_kernel(heads, groups, steps, *refs):
    blocks, refs = refs[: len(steps)], refs[len(steps) :]
    weight_refs, (q_ref, kv_ref) = refs[:6], refs[6:]
    count = blocks[0].shape[0]
    for at, (step, block) in enumerate(zip(steps, blocks)):
        project_block(
            block[...],
            start_of(step, count, groups),
            weight_refs,
            heads,
            q_ref,
            kv_ref,
            slice(at * count, (at + 1) * count),
        )


def project(blocks, steps, weights, heads, groups):
    count, depth = blocks[0].shape
    rows = count * len(blocks)
    return pl.pallas_call(
        functools.partial(project_kernel, heads, groups, steps),
        out_shape=shapes_of(rows, heads),
        cost_estimate=project_cost(rows, depth, heads),
        compiler_params=pltpu.CompilerParams(vmem_limit_bytes=8 * MIB),
        name="project",
    )(*blocks, *weights)


def finish_kernel(heads, groups, steps, last, *refs):
    earlier = refs[: 2 * len(steps)]
    block, *refs = refs[2 * len(steps) :]
    weight_refs, (q_ref, kv_ref) = refs[:6], refs[6:]
    count = block.shape[0]
    me = lax.axis_index("tp")
    for held, part_steps in enumerate(steps):
        for at, step in enumerate(part_steps):
            place = pl.ds(pl.multiple_of((me ^ step) * count, count), count)
            rows = slice(at * count, (at + 1) * count)
            q_ref[place, :] = earlier[2 * held][rows, :]
            kv_ref[place, :] = earlier[2 * held + 1][rows, :]
    project_block(
        block[...],
        start_of(last, count, groups),
        weight_refs,
        heads,
        q_ref,
        kv_ref,
        pl.ds(pl.multiple_of((me ^ last) * count, count), count),
    )


def finish(earlier, steps, block, last, weights, heads, groups):
    count, depth = block.shape
    return pl.pallas_call(
        functools.partial(finish_kernel, heads, groups, steps, last),
        out_shape=shapes_of(count * groups, heads),
        cost_estimate=project_cost(count, depth, heads),
        compiler_params=pltpu.CompilerParams(vmem_limit_bytes=8 * MIB),
        name="finish",
    )(*earlier, block, *weights)


def attend_kernel(heads, pieces, q_ref, *refs):
    kv_refs = refs[:pieces]
    mixing_ref, gain_ref = refs[pieces : pieces + 2]
    hold_ref = refs[-1]
    out_refs = refs[pieces + 2 : -1]
    rows = q_ref.shape[0]
    scale = HEAD ** (-0.5) * log2_e
    for head in range(heads):
        pair = q_ref[:, head * PAIR : (head + 1) * PAIR]
        lane = lax.broadcasted_iota(jnp.int32, pair.shape, 1)
        nothing = jnp.zeros_like(pair)
        both = jnp.concatenate(
            [jnp.where(lane < HEAD, pair, nothing), jnp.where(lane < HEAD, nothing, pair)], axis=0
        )
        base = head * 2 * PAIR

        def scores_of(ref, at, size):
            keys = ref[pl.ds(at, size), base : base + PAIR]
            return lax.dot_general(both, keys, CONTRACT_LAST, preferred_element_type=jnp.float32)

        def summed_of(weights, ref, at, size):
            values = ref[pl.ds(at, size), base + PAIR : base + 2 * PAIR]
            return jnp.dot(
                weights.astype(jnp.bfloat16), values, preferred_element_type=jnp.float32
            )

        if all(ref.shape[0] <= chunk_rows for ref in kv_refs):
            scores = [scores_of(ref, 0, ref.shape[0]) for ref in kv_refs]
            peak = functools.reduce(
                jnp.maximum, [jnp.max(s, axis=1, keepdims=True) for s in scores]
            )
            total = jnp.zeros((2 * rows, 1), jnp.float32)
            summed = jnp.zeros((2 * rows, PAIR), jnp.float32)
            for s, ref in zip(scores, kv_refs):
                weights = jnp.exp2((s - peak) * scale)
                total += jnp.sum(weights, axis=1, keepdims=True)
                summed += summed_of(weights, ref, 0, ref.shape[0])
        else:
            state = (
                jnp.full((2 * rows, 1), floor_value, jnp.float32),
                jnp.zeros((2 * rows, 1), jnp.float32),
                jnp.zeros((2 * rows, PAIR), jnp.float32),
            )
            for ref in kv_refs:
                size = np.gcd(ref.shape[0], chunk_rows).item()

                def step(index, carry, ref=ref, size=size):
                    peak, total, summed = carry
                    at = pl.multiple_of(index * size, size)
                    scores = scores_of(ref, at, size)
                    new_peak = jnp.maximum(peak, jnp.max(scores, axis=1, keepdims=True))
                    factor = jnp.exp2((peak - new_peak) * scale)
                    weights = jnp.exp2((scores - new_peak) * scale)
                    return (
                        new_peak,
                        total * factor + jnp.sum(weights, axis=1, keepdims=True),
                        summed * factor + summed_of(weights, ref, at, size),
                    )

                state = lax.fori_loop(0, ref.shape[0] // size, step, state)
            total, summed = state[1:]
        ratio = summed / total
        mixed = ratio[:rows] - mixing_ref[head] * ratio[rows:]
        square = jnp.mean(mixed * mixed, axis=1, keepdims=True)
        normed = mixed * lax.rsqrt(square + epsilon) * gain_ref[...]
        hold_ref[...] = normed
        me = lax.axis_index("tp")
        share = rows // len(out_refs)
        for step, out_ref in enumerate(out_refs):
            at = pl.multiple_of((me ^ step) * share, share)
            out_ref[:, head * PAIR : (head + 1) * PAIR] = hold_ref[pl.ds(at, share), :].astype(
                jnp.bfloat16
            )


def attend_grant(rows, keys, heads):
    held = 4 * rows * min(keys, chunk_rows) * 8 + 2 * keys * heads * 2 * PAIR
    return held + 8 * MIB


def attend(queries, pieces, mixing, gain, heads, groups):
    rows = queries.shape[0]
    keys = sum(p.shape[0] for p in pieces)
    vmem = pl.BlockSpec(memory_space=pltpu.VMEM)
    return pl.pallas_call(
        functools.partial(attend_kernel, heads, len(pieces)),
        out_shape=[jax.ShapeDtypeStruct((rows // groups, heads * PAIR), jnp.bfloat16)] * groups,
        scratch_shapes=[pltpu.VMEM((rows, PAIR), jnp.float32)],
        in_specs=[vmem] * (1 + len(pieces)) + [pl.BlockSpec(memory_space=pltpu.SMEM), vmem],
        cost_estimate=pl.CostEstimate(
            flops=2 * 4 * rows * keys * heads * PAIR,
            bytes_accessed=2 * keys * heads * 2 * PAIR,
            transcendentals=2 * rows * keys * heads,
        ),
        compiler_params=pltpu.CompilerParams(vmem_limit_bytes=attend_grant(rows, keys, heads)),
        name="attend",
    )(queries, *pieces, mixing, gain.reshape(1, PAIR))


def output_kernel(count, *refs):
    piece_refs = refs[:count]
    weight_ref, out_ref = refs[count:]
    width = piece_refs[0].shape[1]
    me = lax.axis_index("tp")
    total = None
    for step in range(count):
        at = pl.multiple_of((me ^ step) * width, width)
        part = jnp.dot(
            piece_refs[step][...], weight_ref[pl.ds(at, width), :], preferred_element_type=jnp.float32
        )
        total = part if total is None else total + part
    out_ref[...] = total.astype(jnp.bfloat16)


def output(pieces, weight):
    rows, width = pieces[0].shape
    return pl.pallas_call(
        functools.partial(output_kernel, len(pieces)),
        out_shape=jax.ShapeDtypeStruct((rows, weight.shape[1]), jnp.bfloat16),
        cost_estimate=pl.CostEstimate(
            flops=2 * rows * weight.shape[0] * weight.shape[1],
            bytes_accessed=2 * weight.size,
            transcendentals=0,
        ),
        compiler_params=pltpu.CompilerParams(vmem_limit_bytes=8 * MIB),
        name="output",
    )(*pieces, weight)


def exchange(block, axis, step):
    size = lax.axis_size(axis)
    return lax.ppermute(block, axis, [(i, i ^ step) for i in range(size)])


def gather_pieces(packed, axis):
    size = lax.axis_size(axis)
    if size > ring_limit or size & (size - 1):
        return [lax.all_gather(packed, axis, axis=0, tiled=True)]
    half = size // 2
    far = exchange(packed, axis, half)
    near = [exchange(packed, axis, step) for step in range(1, half)]
    forwarded = [exchange(far, axis, step) for step in range(1, half)]
    return [packed, far] + near + forwarded


def per_device(
    tokens, query_one, query_two, key_one, key_two, value_weight, mixing, out_weight, head_gain
):
    groups = lax.axis_size("tp")
    own_rows = tokens.shape[0]
    row_count = own_rows * groups
    heads = query_one.shape[1] // HEAD
    weights = (query_one.T, query_two.T, key_one.T, key_two.T, value_weight)
    across = exchange(tokens, "tp", 2)
    beside = exchange(tokens, "tp", 1)
    own, *held = stage([tokens, *weights])
    across, own = lax.optimization_barrier((across, own))
    last = exchange(across, "tp", 1)
    early = project([own, beside, across], (0, 1, 2), held, heads, groups)
    queries, packed = finish(early, ((0, 1, 2),), last, 3, held, heads, groups)
    pieces = gather_pieces(packed, "sp")
    shares = attend(queries, pieces, mixing, head_gain, heads, groups)
    parts = [exchange(share, "tp", step) if step else share for step, share in enumerate(shares)]
    return output(parts, out_weight)


def solution(mesh):
    in_specs = (
        P(("sp", "tp"), None),
        P(None, "tp"),
        P(None, "tp"),
        P(None, "tp"),
        P(None, "tp"),
        P(None, "tp"),
        P("tp"),
        P(),
        P(),
    )
    out_specs = P(("sp", "tp"), None)
    return jax.shard_map(
        per_device, mesh=mesh, in_specs=in_specs, out_specs=out_specs, check_vma=False
    )
```

time: 60.1 us -> 30.1 us (0.50)
  blocking collectives: 42.4 us -> 0 us
  starting transfers between devices: 0 us -> 14.7 us
  local copies, waits for them, and re-layouts: 10.5 us -> 0.94 us
  waiting for transfers between devices: 0 us -> 8.22 us
  Pallas kernels: 0 us -> 5.34 us
  matrix products: 4.48 us -> 0 us
  other arithmetic: 1.64 us -> 0 us
    all_gather x2 -> x0, blocking collectives: 36.1 us -> none  [the longest x1 27.5 us: per_device(): gathered = lax.all_gather(packed, 'sp', axis=0, tiled=True)]
    ppermute x0 -> x13, starting transfers between devices: none -> 14.7 us  [exchange(): return lax.ppermute(block, axis, [(i, i ^ step) for i in range(size)])]
    ppermute x0 -> x13, waiting for transfers between devices: none -> 8.22 us  [exchange(): return lax.ppermute(block, axis, [(i, i ^ step) for i in range(size)])]
    all_to_all x1 -> x0, blocking collectives: 6.3 us -> none  [per_device(): lax.all_to_all(heads, 'tp', split_axis=0, concat_axis=1, tiled=True)]
    unnamed x12 -> x6, local copies, waits for them, and re-layouts: 6.35 us -> 0.94 us
    pallas_call x0 -> x5, Pallas kernels: none -> 5.34 us  [the longest x1 1.54 us: stage(): pl.pallas_call(functools.partial(stage_kernel, len(arrays)), out_shape=[j...]
    dot_general x6 -> x0, matrix products: 4.48 us -> none  [the longest x1 2.01 us: per_device(): jnp.dot(lax.all_gather(tokens, 'tp', axis=0, tiled=True), joined, preferr...]
    concatenate x2 -> x0, local copies, waits for them, and re-layouts: 4.11 us -> none  [the longest x1 4.1 us: per_device(): jnp.concatenate([query_one, query_two, key_one, key_two, value_weight], a...]
  transfers between devices with their start and end apart: 0 -> 13, of which waited for: 0 -> 9; matrix products, arithmetic and copies ran while one was open for 0% -> 0% of each run, Pallas kernels for 0% -> 9%
where the time goes in v1:
time: 30.1 us; the launch traced here: 30 us
  starting transfers between devices  14.7 us (49%)
  waiting for transfers between devices  8.22 us (27%)
  Pallas kernels  5.34 us (18%)
  local copies, waits for them, and re-layouts  0.94 us (3%)
  between operations  0.71 us (2%)
    ppermute x13, starting transfers between devices, exchange(): return lax.ppermute(block, axis, [(i, i ^ step) for i in range(size)])  14.7 us
    ppermute x13, waiting for transfers between devices, exchange(): return lax.ppermute(block, axis, [(i, i ^ step) for i in range(size)])  8.22 us
    pallas_call x1, Pallas kernels, stage(): pl.pallas_call(functools.partial(stage_kernel, len(arrays)), out_shape=[j...  1.54 us
    pallas_call x1, Pallas kernels, project(): pl.pallas_call(functools.partial(project_kernel, heads, groups, steps), o...  1.23 us
    pallas_call x1, Pallas kernels, output(): pl.pallas_call(functools.partial(output_kernel, len(pieces)), out_shape=j...  1.07 us
    pallas_call x1, Pallas kernels, attend(): pl.pallas_call(functools.partial(attend_kernel, heads, len(pieces)), out_...  0.96 us
    unnamed x6, local copies, waits for them, and re-layouts  0.94 us
  transfers between devices with their start and end apart: 13, of which 9 were waited for; matrix products, arithmetic and copies ran while one was open for 0% of the time, Pallas kernels for 9%

profile of v1, /device:TPU:0, one launch (start us, length us, event | category | flops | bytes accessed | tf_op | source)
XLA Modules:
  0.0 30.0 jit_solution(3419916659549615254)
XLA Ops:
  0.0 3.0 %collective-permute-start = (bf16[32,2048]{1,0:T(8,128)(2,1)}, bf16[32,2048]{1,0:T(8,128)(2,1)S(1)}, u32[]{:S(2)}, u32[]{:S(2)}) collective-permute-start(bf16[32,2048]{1,0:T(8,128)(2,1)} %refs_0_.1), channel_id=1, source_target_pairs={{0,2},{1,3},{2,0},{3,1},{4,6},{5,7},{6,4},{7,5},{8,10},{9,11},{10,... | collective-permute-start | bytes 393224 | tf_op jit(solution)/shard_map/ppermute | solution.py:315
  3.0 0.0 collective-permute-start.1
  3.0 0.0 copy-start.1
  3.0 0.9 %copy-done.1 = bf16[32,2048]{1,0:T(8,128)(2,1)S(1)} copy-done((bf16[32,2048]{1,0:T(8,128)(2,1)S(1)}, bf16[32,2048]{1,0:T(8,128)(2,1)}, u32[]{:S(2)}) %copy-start.1) | copy-done | bytes 131096
  3.9 1.5 %stage.1 = (bf16[32,2048]{1,0:T(8,128)(2,1)S(1)}, bf16[64,2048]{1,0:T(8,128)(2,1)S(1)}, bf16[64,2048]{1,0:T(8,128)(2,1)S(1)}, bf16[64,2048]{1,0:T(8,128)(2,1)S(1...) custom-call(bf16[32,2048]{1,0:T(8,128)(2,1)S(1)} %copy-done.1, ...), custom_call_target="tpu_custom_call" | custom-call | flops 436207616 | bytes 1703936 | tf_op jit(solution)/shard_map/stage/pallas_call | solution.py:111
  5.5 0.0 copy-start.2
  5.5 1.2 %collective-permute-done.refs_2_ = bf16[32,2048]{1,0:T(8,128)(2,1)S(1)} collective-permute-done((bf16[32,2048]{1,0:T(8,128)(2,1)}, bf16[32,2048]{1,0:T(8,128)(2,1)S(1)}, u32[]{:S(2)}, u32[]{:S(2)}) %collective-permute-start) | collective-permute-done | bytes 131104 | tf_op jit(solution)/shard_map/ppermute | solution.py:315
  6.7 0.0 collective-permute-start.2
  6.7 0.0 collective-permute-done.1.refs_1_
  6.7 0.0 copy-start
  6.7 1.2 %project.1 = (bf16[96,128]{1,0:T(8,128)(2,1)S(1)}, bf16[96,256]{1,0:T(8,128)(2,1)S(1)}) custom-call(bf16[32,2048]{1,0:T(8,128)(2,1)S(1)} %get-tuple-element.23.refs_0_, bf16[32,2048]{1,0:T(8,128)(2,1)S(1)} %collective-permute-done.1.refs_1_, bf16[32,2048]{1,0:T(8,128)(2,1)S(1)} %collective-permute-done.refs_2_, ...), custom_call_target="tpu_custom_call" | custom-call | flops 150994944 | tf_op jit(solution)/shard_map/project/pallas_call | solution.py:141
  7.9 0.1 collective-permute-done.2.refs_2_
  8.0 0.5 %finish.1 = (bf16[128,128]{1,0:T(8,128)(2,1)S(1)}, bf16[128,256]{1,0:T(8,128)(2,1)S(1)}) custom-call(bf16[96,128]{1,0:T(8,128)(2,1)S(1)} %get-tuple-element.31.refs_0_, bf16[96,256]{1,0:T(8,128)(2,1)S(1)} %get-tuple-element.32.refs_1_, bf16[32,2048]{1,0:T(8,128)(2,1)S(1)} %collective-permute-done.2.refs_2_, bf16[64,2048]{1,0:T(8,128)(2,1)S(1)} %get-tuple-element.25.refs_3_, ...), custom_call_target="tpu_custom_call" | custom-call | flops 50331648 | tf_op jit(solution)/shard_map/finish/pallas_call | solution.py:175
  8.6 2.9 %collective-permute-start.3 = (bf16[128,256]{1,0:T(8,128)(2,1)S(1)}, bf16[128,256]{1,0:T(8,128)(2,1)S(1)}, u32[]{:S(2)}, u32[]{:S(2)}) collective-permute-start(bf16[128,256]{1,0:T(8,128)(2,1)S(1)} %get-tuple-element.34.refs_0_), channel_id=1, source_target_pairs={{0,16},{4,20},{8,24},{12,28},{16,0},{20,4},{24,8},{28,12},{1,17},{... | collective-permute-start | bytes 196616 | tf_op jit(solution)/shard_map/ppermute | solution.py:315
  11.4 1.5 %collective-permute-start.4 = (bf16[128,256]{1,0:T(8,128)(2,1)S(1)}, bf16[128,256]{1,0:T(8,128)(2,1)S(1)}, u32[]{:S(2)}, u32[]{:S(2)}) collective-permute-start(bf16[128,256]{1,0:T(8,128)(2,1)S(1)} %get-tuple-element.34.refs_0_), channel_id=1, source_target_pairs={{0,4},{4,0},{8,12},{12,8},{16,20},{20,16},{24,28},{28,24},{1,5},{5... | collective-permute-start | bytes 196616 | tf_op jit(solution)/shard_map/ppermute | solution.py:315
  13.0 1.6 %collective-permute-start.5 = (bf16[128,256]{1,0:T(8,128)(2,1)S(1)}, bf16[128,256]{1,0:T(8,128)(2,1)S(1)}, u32[]{:S(2)}, u32[]{:S(2)}) collective-permute-start(bf16[128,256]{1,0:T(8,128)(2,1)S(1)} %get-tuple-element.34.refs_0_), channel_id=1, source_target_pairs={{0,8},{4,12},{8,0},{12,4},{16,24},{20,28},{24,16},{28,20},{1,9},{5... | collective-permute-start | bytes 196616 | tf_op jit(solution)/shard_map/ppermute | solution.py:315
  14.5 0.4 %collective-permute-start.6 = (bf16[128,256]{1,0:T(8,128)(2,1)S(1)}, bf16[128,256]{1,0:T(8,128)(2,1)S(1)}, u32[]{:S(2)}, u32[]{:S(2)}) collective-permute-start(bf16[128,256]{1,0:T(8,128)(2,1)S(1)} %get-tuple-element.34.refs_0_), channel_id=1, source_target_pairs={{0,12},{4,8},{8,4},{12,0},{16,28},{20,24},{24,20},{28,16},{1,13},{... | collective-permute-start | bytes 196616 | tf_op jit(solution)/shard_map/ppermute | solution.py:315
  14.9 0.6 %collective-permute-done.3.refs_1_ = bf16[128,256]{1,0:T(8,128)(2,1)S(1)} collective-permute-done((bf16[128,256]{1,0:T(8,128)(2,1)S(1)}, bf16[128,256]{1,0:T(8,128)(2,1)S(1)}, u32[]{:S(2)}, u32[]{:S(2)}) %collective-permute-start.3) | collective-permute-done | bytes 65568 | tf_op jit(solution)/shard_map/ppermute | solution.py:315
  15.5 1.4 %collective-permute-start.7 = (bf16[128,256]{1,0:T(8,128)(2,1)S(1)}, bf16[128,256]{1,0:T(8,128)(2,1)S(1)}, u32[]{:S(2)}, u32[]{:S(2)}) collective-permute-start(bf16[128,256]{1,0:T(8,128)(2,1)S(1)} %collective-permute-done.3.refs_1_), channel_id=1, source_target_pairs={{0,4},{4,0},{8,12},{12,8},{16,20},{20,16},{24,28},{28,24},{1,5},{5... | collective-permute-start | bytes 196616 | tf_op jit(solution)/shard_map/ppermute | solution.py:315
  16.9 1.1 %collective-permute-start.8 = (bf16[128,256]{1,0:T(8,128)(2,1)S(1)}, bf16[128,256]{1,0:T(8,128)(2,1)S(1)}, u32[]{:S(2)}, u32[]{:S(2)}) collective-permute-start(bf16[128,256]{1,0:T(8,128)(2,1)S(1)} %collective-permute-done.3.refs_1_), channel_id=1, source_target_pairs={{0,8},{4,12},{8,0},{12,4},{16,24},{20,28},{24,16},{28,20},{1,9},{5... | collective-permute-start | bytes 196616 | tf_op jit(solution)/shard_map/ppermute | solution.py:315
  18.0 0.0 collective-permute-done.4.refs_2_
  18.0 1.0 %collective-permute-start.9 = (bf16[128,256]{1,0:T(8,128)(2,1)S(1)}, bf16[128,256]{1,0:T(8,128)(2,1)S(1)}, u32[]{:S(2)}, u32[]{:S(2)}) collective-permute-start(bf16[128,256]{1,0:T(8,128)(2,1)S(1)} %collective-permute-done.3.refs_1_), channel_id=1, source_target_pairs={{0,12},{4,8},{8,4},{12,0},{16,28},{20,24},{24,20},{28,16},{1,13},{... | collective-permute-start | bytes 196616 | tf_op jit(solution)/shard_map/ppermute | solution.py:315
  19.7 0.0 collective-permute-done.5.refs_3_
  19.7 0.2 collective-permute-done.6.refs_4_
  19.9 0.6 %collective-permute-done.7.refs_5_ = bf16[128,256]{1,0:T(8,128)(2,1)S(1)} collective-permute-done((bf16[128,256]{1,0:T(8,128)(2,1)S(1)}, bf16[128,256]{1,0:T(8,128)(2,1)S(1)}, u32[]{:S(2)}, u32[]{:S(2)}) %collective-permute-start.7) | collective-permute-done | bytes 65568 | tf_op jit(solution)/shard_map/ppermute | solution.py:315
  20.5 0.8 %collective-permute-done.8.refs_6_ = bf16[128,256]{1,0:T(8,128)(2,1)S(1)} collective-permute-done((bf16[128,256]{1,0:T(8,128)(2,1)S(1)}, bf16[128,256]{1,0:T(8,128)(2,1)S(1)}, u32[]{:S(2)}, u32[]{:S(2)}) %collective-permute-start.8) | collective-permute-done | bytes 65568 | tf_op jit(solution)/shard_map/ppermute | solution.py:315
  21.2 2.0 %collective-permute-done.9.refs_7_ = bf16[128,256]{1,0:T(8,128)(2,1)S(1)} collective-permute-done((bf16[128,256]{1,0:T(8,128)(2,1)S(1)}, bf16[128,256]{1,0:T(8,128)(2,1)S(1)}, u32[]{:S(2)}, u32[]{:S(2)}) %collective-permute-start.9) | collective-permute-done | bytes 65568 | tf_op jit(solution)/shard_map/ppermute | solution.py:315
  23.2 0.0 copy-done.2
  23.2 1.0 %attend.1 = (bf16[32,128]{1,0:T(8,128)(2,1)S(1)}, bf16[32,128]{1,0:T(8,128)(2,1)S(1)}, bf16[32,128]{1,0:T(8,128)(2,1)S(1)}, bf16[32,128]{1,0:T(8,128)(2,1)S(1)}) custom-call(bf16[128,128]{1,0:T(8,128)(2,1)S(1)} %get-tuple-element.33.q_ref, bf16[128,256]{1,0:T(8,128)(2,1)S(1)} %get-tuple-element.34.refs_0_, ...), custom_call_target="tpu_custom_call" | custom-call | flops 134217728 | bytes 524288 | tf_op jit(solution)/shard_map/attend/pallas_call | solution.py:268
  24.2 0.1 collective-permute-start.10
  24.3 1.6 %collective-permute-start.11 = (bf16[32,128]{1,0:T(8,128)(2,1)S(1)}, bf16[32,128]{1,0:T(8,128)(2,1)S(1)}, u32[]{:S(2)}, u32[]{:S(2)}) collective-permute-start(bf16[32,128]{1,0:T(8,128)(2,1)S(1)} %get-tuple-element.37), channel_id=1, source_target_pairs={{0,2},{1,3},{2,0},{3,1},{4,6},{5,7},{6,4},{7,5},{8,10},{9,11},{10,... | collective-permute-start | bytes 24584 | tf_op jit(solution)/shard_map/ppermute | solution.py:315
  25.8 0.3 collective-permute-start.12
  26.1 0.0 collective-permute-done.10.refs_1_
  26.1 1.9 %collective-permute-done.11.refs_2_ = bf16[32,128]{1,0:T(8,128)(2,1)S(1)} collective-permute-done((bf16[32,128]{1,0:T(8,128)(2,1)S(1)}, bf16[32,128]{1,0:T(8,128)(2,1)S(1)}, u32[]{:S(2)}, u32[]{:S(2)}) %collective-permute-start.11) | collective-permute-done | bytes 8224 | tf_op jit(solution)/shard_map/ppermute | solution.py:315
  28.0 0.9 %collective-permute-done.12.refs_3_ = bf16[32,128]{1,0:T(8,128)(2,1)S(1)} collective-permute-done((bf16[32,128]{1,0:T(8,128)(2,1)S(1)}, bf16[32,128]{1,0:T(8,128)(2,1)S(1)}, u32[]{:S(2)}, u32[]{:S(2)}) %collective-permute-start.12) | collective-permute-done | bytes 8224 | tf_op jit(solution)/shard_map/ppermute | solution.py:315
  28.9 0.0 copy-done
  28.9 1.1 %output.1 = bf16[32,2048]{1,0:T(8,128)(2,1)} custom-call(bf16[32,128]{1,0:T(8,128)(2,1)S(1)} %get-tuple-element.35.refs_0_, bf16[32,128]{1,0:T(8,128)(2,1)S(1)} %collective-permute-done.10.refs_1_, bf16[32,128]{1,0:T(8,128)(2,1)S(1)} %collective-permute-done.11.refs_2_, bf16[32,128]{1,0:T(8,128)(2,1)S(1)} %collective-permute-done.12.refs_3_, ...), custom_call_target="tpu_custom_call" | custom-call | flops 67108864 | bytes 2097152 | tf_op jit(solution)/shard_map/output/pallas_call | solution.py:300
Async XLA Ops:
  0.0 6.7 %collective-permute-start = (bf16[32,2048]{1,0:T(8,128)(2,1)}, bf16[32,2048]{1,0:T(8,128)(2,1)S(1)}, u32[]{:S(2)}, u32[]{:S(2)}) collective-permute-start(bf16[32,2048]{1,0:T(8,128)(2,1)} %refs_0_.1), channel_id=1, source_target_pairs={{0,2},{1,3},{2,0},{3,1},{4,6},{5,7},{6,4},{7,5},{8,10},{9,11},{10,... | collective-permute-start | bytes 393224 | tf_op jit(solution)/shard_map/ppermute | solution.py:315
  3.0 3.7 %collective-permute-start.1 = (bf16[32,2048]{1,0:T(8,128)(2,1)}, bf16[32,2048]{1,0:T(8,128)(2,1)S(1)}, u32[]{:S(2)}, u32[]{:S(2)}) collective-permute-start(bf16[32,2048]{1,0:T(8,128)(2,1)} %refs_0_.1), channel_id=1, source_target_pairs={{0,1},{1,0},{2,3},{3,2},{4,5},{5,4},{6,7},{7,6},{8,9},{9,8},{10,11... | collective-permute-start | bytes 393224 | tf_op jit(solution)/shard_map/ppermute | solution.py:315
  3.0 0.9 %copy-start.1 = (bf16[32,2048]{1,0:T(8,128)(2,1)S(1)}, bf16[32,2048]{1,0:T(8,128)(2,1)}, u32[]{:S(2)}) copy-start(bf16[32,2048]{1,0:T(8,128)(2,1)} %refs_0_.1) | copy-start | bytes 393220
  5.5 17.8 %copy-start.2 = (f32[128]{0:T(128)S(1)}, f32[128]{0:T(128)}, u32[]{:S(2)}) copy-start(f32[128]{0:T(128)} %param.17) | copy-start | bytes 1540
  6.7 1.3 %collective-permute-start.2 = (bf16[32,2048]{1,0:T(8,128)(2,1)S(1)}, bf16[32,2048]{1,0:T(8,128)(2,1)S(1)}, u32[]{:S(2)}, u32[]{:S(2)}) collective-permute-start(bf16[32,2048]{1,0:T(8,128)(2,1)S(1)} %collective-permute-done.refs_2_), channel_id=1, source_target_pairs={{0,1},{1,0},{2,3},{3,2},{4,5},{5,4},{6,7},{7,6},{8,9},{9,8},{10,11... | collective-permute-start | bytes 393224 | tf_op jit(solution)/shard_map/ppermute | solution.py:315
  6.7 22.2 %copy-start = (bf16[512,2048]{1,0:T(8,128)(2,1)S(1)}, bf16[512,2048]{1,0:T(8,128)(2,1)}, u32[]{:S(2)}) copy-start(bf16[512,2048]{1,0:T(8,128)(2,1)} %refs_4_.1) | copy-start | bytes 6291460
  8.6 7.0 %collective-permute-start.3 = (bf16[128,256]{1,0:T(8,128)(2,1)S(1)}, bf16[128,256]{1,0:T(8,128)(2,1)S(1)}, u32[]{:S(2)}, u32[]{:S(2)}) collective-permute-start(bf16[128,256]{1,0:T(8,128)(2,1)S(1)} %get-tuple-element.34.refs_0_), channel_id=1, source_target_pairs={{0,16},{4,20},{8,24},{12,28},{16,0},{20,4},{24,8},{28,12},{1,17},{... | collective-permute-start | bytes 196616 | tf_op jit(solution)/shard_map/ppermute | solution.py:315
  11.4 6.6 %collective-permute-start.4 = (bf16[128,256]{1,0:T(8,128)(2,1)S(1)}, bf16[128,256]{1,0:T(8,128)(2,1)S(1)}, u32[]{:S(2)}, u32[]{:S(2)}) collective-permute-start(bf16[128,256]{1,0:T(8,128)(2,1)S(1)} %get-tuple-element.34.refs_0_), channel_id=1, source_target_pairs={{0,4},{4,0},{8,12},{12,8},{16,20},{20,16},{24,28},{28,24},{1,5},{5... | collective-permute-start | bytes 196616 | tf_op jit(solution)/shard_map/ppermute | solution.py:315
  13.0 6.7 %collective-permute-start.5 = (bf16[128,256]{1,0:T(8,128)(2,1)S(1)}, bf16[128,256]{1,0:T(8,128)(2,1)S(1)}, u32[]{:S(2)}, u32[]{:S(2)}) collective-permute-start(bf16[128,256]{1,0:T(8,128)(2,1)S(1)} %get-tuple-element.34.refs_0_), channel_id=1, source_target_pairs={{0,8},{4,12},{8,0},{12,4},{16,24},{20,28},{24,16},{28,20},{1,9},{5... | collective-permute-start | bytes 196616 | tf_op jit(solution)/shard_map/ppermute | solution.py:315
  14.5 5.3 %collective-permute-start.6 = (bf16[128,256]{1,0:T(8,128)(2,1)S(1)}, bf16[128,256]{1,0:T(8,128)(2,1)S(1)}, u32[]{:S(2)}, u32[]{:S(2)}) collective-permute-start(bf16[128,256]{1,0:T(8,128)(2,1)S(1)} %get-tuple-element.34.refs_0_), channel_id=1, source_target_pairs={{0,12},{4,8},{8,4},{12,0},{16,28},{20,24},{24,20},{28,16},{1,13},{... | collective-permute-start | bytes 196616 | tf_op jit(solution)/shard_map/ppermute | solution.py:315
  15.5 4.9 %collective-permute-start.7 = (bf16[128,256]{1,0:T(8,128)(2,1)S(1)}, bf16[128,256]{1,0:T(8,128)(2,1)S(1)}, u32[]{:S(2)}, u32[]{:S(2)}) collective-permute-start(bf16[128,256]{1,0:T(8,128)(2,1)S(1)} %collective-permute-done.3.refs_1_), channel_id=1, source_target_pairs={{0,4},{4,0},{8,12},{12,8},{16,20},{20,16},{24,28},{28,24},{1,5},{5... | collective-permute-start | bytes 196616 | tf_op jit(solution)/shard_map/ppermute | solution.py:315
  16.9 4.3 %collective-permute-start.8 = (bf16[128,256]{1,0:T(8,128)(2,1)S(1)}, bf16[128,256]{1,0:T(8,128)(2,1)S(1)}, u32[]{:S(2)}, u32[]{:S(2)}) collective-permute-start(bf16[128,256]{1,0:T(8,128)(2,1)S(1)} %collective-permute-done.3.refs_1_), channel_id=1, source_target_pairs={{0,8},{4,12},{8,0},{12,4},{16,24},{20,28},{24,16},{28,20},{1,9},{5... | collective-permute-start | bytes 196616 | tf_op jit(solution)/shard_map/ppermute | solution.py:315
  18.0 5.2 %collective-permute-start.9 = (bf16[128,256]{1,0:T(8,128)(2,1)S(1)}, bf16[128,256]{1,0:T(8,128)(2,1)S(1)}, u32[]{:S(2)}, u32[]{:S(2)}) collective-permute-start(bf16[128,256]{1,0:T(8,128)(2,1)S(1)} %collective-permute-done.3.refs_1_), channel_id=1, source_target_pairs={{0,12},{4,8},{8,4},{12,0},{16,28},{20,24},{24,20},{28,16},{1,13},{... | collective-permute-start | bytes 196616 | tf_op jit(solution)/shard_map/ppermute | solution.py:315
  24.2 1.9 %collective-permute-start.10 = (bf16[32,128]{1,0:T(8,128)(2,1)S(1)}, bf16[32,128]{1,0:T(8,128)(2,1)S(1)}, u32[]{:S(2)}, u32[]{:S(2)}) collective-permute-start(bf16[32,128]{1,0:T(8,128)(2,1)S(1)} %get-tuple-element.36), channel_id=1, source_target_pairs={{0,1},{1,0},{2,3},{3,2},{4,5},{5,4},{6,7},{7,6},{8,9},{9,8},{10,11... | collective-permute-start | bytes 24584 | tf_op jit(solution)/shard_map/ppermute | solution.py:315
  24.3 3.7 %collective-permute-start.11 = (bf16[32,128]{1,0:T(8,128)(2,1)S(1)}, bf16[32,128]{1,0:T(8,128)(2,1)S(1)}, u32[]{:S(2)}, u32[]{:S(2)}) collective-permute-start(bf16[32,128]{1,0:T(8,128)(2,1)S(1)} %get-tuple-element.37), channel_id=1, source_target_pairs={{0,2},{1,3},{2,0},{3,1},{4,6},{5,7},{6,4},{7,5},{8,10},{9,11},{10,... | collective-permute-start | bytes 24584 | tf_op jit(solution)/shard_map/ppermute | solution.py:315
  25.8 3.1 %collective-permute-start.12 = (bf16[32,128]{1,0:T(8,128)(2,1)S(1)}, bf16[32,128]{1,0:T(8,128)(2,1)S(1)}, u32[]{:S(2)}, u32[]{:S(2)}) collective-permute-start(bf16[32,128]{1,0:T(8,128)(2,1)S(1)} %get-tuple-element.38), channel_id=1, source_target_pairs={{0,3},{1,2},{2,1},{3,0},{4,7},{5,6},{6,5},{7,4},{8,11},{9,10},{10,... | collective-permute-start | bytes 24584 | tf_op jit(solution)/shard_map/ppermute | solution.py:315

commit v2 on v1

v2 whole, which is shorter than its diff:
```python
import functools

import jax
import jax.numpy as jnp
import numpy as np
from jax import lax
from jax.experimental import pallas as pl
from jax.experimental.pallas import tpu as pltpu
from jax.sharding import PartitionSpec as P

HEAD = 64
GRID_W = 64
PAIR = 2 * HEAD

epsilon = 1e-06
theta_base = 10000.0
floor_value = -1e30
ring_limit = 16
chunk_rows = 1024
log2_e = 1.4426950408889634
MIB = 1 << 20
stage_grant = 52 * MIB

CONTRACT_LAST = (((1,), (1,)), ((), ()))


def turn_of(start, count):
    quarter = HEAD // 4
    lane = lax.broadcasted_iota(jnp.int32, (1, PAIR), 1)
    index = lane % quarter
    freqs = jnp.zeros((1, PAIR), jnp.float32)
    for j in range(quarter):
        freqs = jnp.where(index == j, theta_base ** (-j / quarter), freqs)
    token = start + lax.broadcasted_iota(jnp.int32, (count, PAIR), 0)
    by_row = (lane & (HEAD // 2)) == 0
    position = jnp.where(by_row, token // GRID_W, token % GRID_W).astype(jnp.float32)
    angle = position * freqs
    sine = jnp.sin(angle)
    return jnp.cos(angle), jnp.where((lane & quarter) == 0, -sine, sine)


def turned(field, cosine, sine):
    lane = lax.broadcasted_iota(jnp.int32, field.shape, 1)
    ahead = pltpu.roll(field, PAIR - HEAD // 4, 1)
    behind = pltpu.roll(field, HEAD // 4, 1)
    partner = jnp.where((lane & (HEAD // 4)) == 0, ahead, behind)
    return (field * cosine + partner * sine).astype(jnp.bfloat16)


def project_blocks(blocks, places, weight_refs, heads, q_ref, kv_ref, place):
    one_q, two_q, one_k, two_k, upper, lower, cosine_ref, sine_ref = weight_refs
    count = blocks[0].shape[0]
    tokens = jnp.concatenate([block[...] for block in blocks], axis=0)
    cosine, sine = [
        jnp.concatenate([ref[pl.ds(at, count), :] for at in places], axis=0)
        for ref in (cosine_ref, sine_ref)
    ]
    half = upper.shape[0]
    for head in range(heads):
        rows = slice(head * HEAD, (head + 1) * HEAD)
        columns = slice(head * PAIR, (head + 1) * PAIR)
        base = head * 2 * PAIR

        def turned_pair(first, second):
            joined = jnp.concatenate([first[rows, :], second[rows, :]], axis=0)
            pair = lax.dot_general(
                tokens, joined, CONTRACT_LAST, preferred_element_type=jnp.float32
            )
            return turned(pair, cosine, sine)

        if kv_ref is not None:
            kv_ref[place, base : base + PAIR] = turned_pair(one_k, two_k)
            values = jnp.dot(
                tokens[:, :half], upper[:, columns], preferred_element_type=jnp.float32
            ) + jnp.dot(tokens[:, half:], lower[:, columns], preferred_element_type=jnp.float32)
            kv_ref[place, base + PAIR : base + 2 * PAIR] = values.astype(jnp.bfloat16)
        if q_ref is not None:
            q_ref[place, columns] = turned_pair(one_q, two_q)


def place_of(step, count):
    return pl.multiple_of((lax.axis_index("tp") ^ step) * count, count)


def stage_kernel(count, *refs):
    sources, held, (cosine_ref, sine_ref, sems) = refs[:count], refs[count:-3], refs[-3:]
    half = sources[-1].shape[0] // 2
    sources = [*sources[:-1], sources[-1].at[pl.ds(0, half)], sources[-1].at[pl.ds(half, half)]]
    copies = [pltpu.make_async_copy(a, b, sems.at[i]) for i, (a, b) in enumerate(zip(sources, held))]
    for copy in copies:
        copy.start()
    rows = cosine_ref.shape[0]
    cosine_ref[...], sine_ref[...] = turn_of(lax.axis_index("sp") * rows, rows)
    for copy in copies:
        copy.wait()


def shapes_of(rows, heads):
    return [
        jax.ShapeDtypeStruct((rows, heads * PAIR), jnp.bfloat16),
        jax.ShapeDtypeStruct((rows, heads * 2 * PAIR), jnp.bfloat16),
    ]


def project_cost(rows, depth, heads):
    return pl.CostEstimate(
        flops=2 * rows * depth * heads * 3 * PAIR, bytes_accessed=0, transcendentals=0
    )


def stage(arrays, total):
    size = sum(a.size * 2 for a in arrays)
    rows, columns = arrays[-1].shape
    shapes = [a.shape for a in arrays[:-1]] + [(rows // 2, columns)] * 2
    return pl.pallas_call(
        functools.partial(stage_kernel, len(arrays)),
        out_shape=[jax.ShapeDtypeStruct(shape, arrays[0].dtype) for shape in shapes]
        + [jax.ShapeDtypeStruct((total, PAIR), jnp.float32)] * 2,
        in_specs=[pl.BlockSpec(memory_space=pltpu.HBM)] * len(arrays),
        scratch_shapes=[pltpu.SemaphoreType.DMA((len(shapes),))],
        cost_estimate=pl.CostEstimate(flops=size * 256, bytes_accessed=size, transcendentals=0),
        compiler_params=pltpu.CompilerParams(vmem_limit_bytes=stage_grant),
        name="stage",
    )(*arrays)


def project_kernel(heads, steps, *refs):
    blocks, refs = refs[: len(steps)], refs[len(steps) :]
    weight_refs, (q_ref, kv_ref) = refs[:8], refs[8:]
    places = [place_of(step, blocks[0].shape[0]) for step in steps]
    project_blocks(blocks, places, weight_refs, heads, q_ref, kv_ref, slice(None))


def project(blocks, steps, weights, heads):
    count, depth = blocks[0].shape
    rows = count * len(blocks)
    return pl.pallas_call(
        functools.partial(project_kernel, heads, steps),
        out_shape=shapes_of(rows, heads),
        cost_estimate=project_cost(rows, depth, heads),
        compiler_params=pltpu.CompilerParams(vmem_limit_bytes=8 * MIB),
        name="project",
    )(*blocks, *weights)


def finish_kernel(heads, steps, last, keys, early_ref, block_ref, *refs):
    weight_refs, out_ref = refs[:8], refs[8]
    count = block_ref.shape[0]
    for at, step in enumerate(steps):
        out_ref[pl.ds(place_of(step, count), count), :] = early_ref[at * count : (at + 1) * count, :]
    place = place_of(last, count)
    project_blocks(
        [block_ref],
        [place],
        weight_refs,
        heads,
        None if keys else out_ref,
        out_ref if keys else None,
        pl.ds(place, count),
    )


def finish(early, steps, block, last, weights, heads, groups, keys):
    count, depth = block.shape
    return pl.pallas_call(
        functools.partial(finish_kernel, heads, steps, last, keys),
        out_shape=jax.ShapeDtypeStruct((count * groups, early.shape[1]), early.dtype),
        cost_estimate=project_cost(count, depth, heads),
        compiler_params=pltpu.CompilerParams(vmem_limit_bytes=8 * MIB),
        name="keys" if keys else "queries",
    )(early, block, *weights)


def both_of(pair):
    lane = lax.broadcasted_iota(jnp.int32, pair.shape, 1)
    nothing = jnp.zeros_like(pair)
    return jnp.concatenate(
        [jnp.where(lane < HEAD, pair, nothing), jnp.where(lane < HEAD, nothing, pair)], axis=0
    )


def absorb(state, both, kv_refs, head):
    scale = HEAD ** (-0.5) * log2_e
    base = head * 2 * PAIR

    def taken(carry, parts):
        scores = [
            lax.dot_general(
                both,
                ref[rows, base : base + PAIR],
                CONTRACT_LAST,
                preferred_element_type=jnp.float32,
            )
            for ref, rows in parts
        ]
        peaks = [jnp.max(s, axis=1, keepdims=True) for s in scores]
        if carry is None:
            peak, total, summed = functools.reduce(jnp.maximum, peaks), None, None
        else:
            before, total, summed = carry
            peak = functools.reduce(jnp.maximum, peaks, before)
            factor = jnp.exp2((before - peak) * scale)
            total, summed = total * factor, summed * factor
        for s, (ref, rows) in zip(scores, parts):
            weights = jnp.exp2((s - peak) * scale)
            partial = jnp.sum(weights, axis=1, keepdims=True)
            product = jnp.dot(
                weights.astype(jnp.bfloat16),
                ref[rows, base + PAIR : base + 2 * PAIR],
                preferred_element_type=jnp.float32,
            )
            total = partial if total is None else total + partial
            summed = product if summed is None else summed + product
        return peak, total, summed

    if sum(ref.shape[0] for ref in kv_refs) <= chunk_rows:
        return taken(state, [(ref, slice(None)) for ref in kv_refs])
    for ref in kv_refs:
        size = np.gcd(ref.shape[0], chunk_rows).item()
        if state is None:
            rows = both.shape[0]
            state = (
                jnp.full((rows, 1), floor_value, jnp.float32),
                jnp.zeros((rows, 1), jnp.float32),
                jnp.zeros((rows, PAIR), jnp.float32),
            )

        def step(index, carry, ref=ref, size=size):
            return taken(carry, [(ref, pl.ds(pl.multiple_of(index * size, size), size))])

        state = lax.fori_loop(0, ref.shape[0] // size, step, state)
    return state


def begin_kernel(heads, pieces, held, q_ref, *refs):
    state_refs, kv_refs, out_refs = refs[:held], refs[held : held + pieces], refs[held + pieces :]
    for head in range(heads):
        state = tuple(ref[head] for ref in state_refs) or None
        both = both_of(q_ref[:, head * PAIR : (head + 1) * PAIR])
        for ref, value in zip(out_refs, absorb(state, both, kv_refs, head)):
            ref[head] = value


def attend_kernel(heads, pieces, held, groups, steps, q_ref, *refs):
    state_refs, refs = refs[:held], refs[held:]
    kv_refs, (mixing_ref, gain_ref), out_refs = refs[:pieces], refs[pieces : pieces + 2], refs[pieces + 2 :]
    total_rows = q_ref.shape[0]
    share = total_rows // groups
    rows = share * len(steps)
    places = [place_of(step, share) for step in steps]
    for head in range(heads):
        columns = slice(head * PAIR, (head + 1) * PAIR)
        pair = jnp.concatenate([q_ref[pl.ds(at, share), columns] for at in places], axis=0)
        state = None
        if held:
            spots = places + [total_rows + at for at in places]
            state = tuple(
                jnp.concatenate([ref[head, pl.ds(at, share), :] for at in spots], axis=0)
                for ref in state_refs
            )
        _, total, summed = absorb(state, both_of(pair), kv_refs, head)
        ratio = summed / total
        mixed = ratio[:rows] - mixing_ref[:, head : head + 1] * ratio[rows:]
        square = jnp.mean(mixed * mixed, axis=1, keepdims=True)
        normed = (mixed * lax.rsqrt(square + epsilon) * gain_ref[...]).astype(jnp.bfloat16)
        for at, out_ref in enumerate(out_refs):
            out_ref[:, columns] = normed[at * share : (at + 1) * share]


def attend_grant(rows, keys, heads):
    return 4 * rows * min(keys, chunk_rows) * 8 + 2 * keys * heads * 2 * PAIR + 8 * MIB


def attend_cost(rows, keys, heads):
    return pl.CostEstimate(
        flops=2 * 4 * rows * keys * heads * PAIR,
        bytes_accessed=0,
        transcendentals=2 * rows * keys * heads,
    )


def begin(queries, state, pieces, heads):
    rows = queries.shape[0]
    keys = sum(p.shape[0] for p in pieces)
    return pl.pallas_call(
        functools.partial(begin_kernel, heads, len(pieces), len(state)),
        out_shape=[
            jax.ShapeDtypeStruct((heads, 2 * rows, width), jnp.float32) for width in (1, 1, PAIR)
        ],
        cost_estimate=attend_cost(rows, keys, heads),
        compiler_params=pltpu.CompilerParams(vmem_limit_bytes=attend_grant(rows, keys, heads)),
        name="middle" if state else "begin",
    )(queries, *state, *pieces)


def attend(queries, state, pieces, mixing, gain, heads, groups, steps):
    rows = queries.shape[0]
    keys = sum(p.shape[0] for p in pieces)
    share = jax.ShapeDtypeStruct((rows // groups, heads * PAIR), jnp.bfloat16)
    return pl.pallas_call(
        functools.partial(attend_kernel, heads, len(pieces), len(state), groups, steps),
        out_shape=[share] * len(steps),
        cost_estimate=attend_cost(rows * len(steps) // groups, keys, heads),
        compiler_params=pltpu.CompilerParams(vmem_limit_bytes=attend_grant(rows, keys, heads)),
        name="attend",
    )(queries, *state, *pieces, mixing.reshape(1, heads), gain.reshape(1, PAIR))


def summed_shares(share_refs, steps, weight_ref, total):
    width = share_refs[0].shape[1]
    for step, ref in zip(steps, share_refs):
        part = jnp.dot(
            ref[...],
            weight_ref[pl.ds(place_of(step, width), width), :],
            preferred_element_type=jnp.float32,
        )
        total = part if total is None else total + part
    return total


def output_kernel(steps, held, *refs):
    share_refs, weight_ref, out_ref = refs[held : held + len(steps)], refs[-2], refs[-1]
    total = summed_shares(share_refs, steps, weight_ref, refs[0][...] if held else None)
    out_ref[...] = total.astype(out_ref.dtype)


def output(earlier, shares, steps, weight, dtype):
    rows, width = shares[0].shape
    return pl.pallas_call(
        functools.partial(output_kernel, steps, len(earlier)),
        out_shape=jax.ShapeDtypeStruct((rows, weight.shape[1]), dtype),
        cost_estimate=pl.CostEstimate(
            flops=2 * rows * width * len(steps) * weight.shape[1],
            bytes_accessed=0,
            transcendentals=0,
        ),
        compiler_params=pltpu.CompilerParams(vmem_limit_bytes=8 * MIB),
        name="output" if earlier else "early",
    )(*earlier, *shares, weight)


def exchange(block, axis, step):
    size = lax.axis_size(axis)
    return lax.ppermute(block, axis, [(i, i ^ step) for i in range(size)])


def gather_pieces(packed, axis):
    size = lax.axis_size(axis)
    if size > ring_limit or size & (size - 1):
        return [], [lax.all_gather(packed, axis, axis=0, tiled=True)]
    half = size // 2
    far = exchange(packed, axis, half)
    near = [exchange(packed, axis, step) for step in range(half - 1, 0, -1)]
    forwarded = [exchange(far, axis, step) for step in range(half - 1, 0, -1)]
    return [packed, far] + near, forwarded


def per_device(
    tokens, query_one, query_two, key_one, key_two, value_weight, mixing, out_weight, head_gain
):
    groups = lax.axis_size("tp")
    own_rows = tokens.shape[0]
    row_count = own_rows * groups
    heads = query_one.shape[1] // HEAD
    weights = (query_one.T, query_two.T, key_one.T, key_two.T, value_weight)
    across = exchange(tokens, "tp", 2)
    beside = exchange(tokens, "tp", 1)
    own, *held = stage([tokens, *weights], own_rows * groups)
    across, own = lax.optimization_barrier((across, own))
    last = exchange(across, "tp", 1)
    early = project([own, beside, across], (0, 1, 2), held, heads)
    packed = finish(early[1], (0, 1, 2), last, 3, held, heads, groups, True)
    queries = finish(early[0], (0, 1, 2), last, 3, held, heads, groups, False)
    first, second = gather_pieces(packed, "sp")
    state = begin(queries, [], first, heads) if first else []
    if len(second) > 1:
        state, second = begin(queries, state, second[:-1], heads), second[-1:]
    rest = (mixing, head_gain, heads, groups)
    own, beside, across, aside = attend(queries, state, second, *rest, (0, 1, 2, 3))
    across, aside = exchange(across, "tp", 2), exchange(aside, "tp", 3)
    beside = exchange(beside, "tp", 1)
    early = output([], [own, aside], (0, 3), out_weight, jnp.float32)
    return output([early], [across, beside], (2, 1), out_weight, jnp.bfloat16)


def solution(mesh):
    in_specs = (
        P(("sp", "tp"), None),
        P(None, "tp"),
        P(None, "tp"),
        P(None, "tp"),
        P(None, "tp"),
        P(None, "tp"),
        P("tp"),
        P(),
        P(),
    )
    out_specs = P(("sp", "tp"), None)
    return jax.shard_map(
        per_device, mesh=mesh, in_specs=in_specs, out_specs=out_specs, check_vma=False
    )
```

time: 30.1 us -> 27.8 us (0.924)
  waiting for transfers between devices: 8.22 us -> 5.19 us
  Pallas kernels: 5.34 us -> 5.94 us
    ppermute x13, waiting for transfers between devices: 8.22 us -> 5.19 us  [exchange(): return lax.ppermute(block, axis, [(i, i ^ step) for i in range(size)])]
    pallas_call x4 -> x8, Pallas kernels: 3.8 us -> 4.4 us  [the longest x2 1.21 us: begin(): pl.pallas_call(functools.partial(begin_kernel, heads, len(pieces), len(st...]
  transfers between devices with their start and end apart: 13 -> 13, of which waited for: 9 -> 8; matrix products, arithmetic and copies ran while one was open for 0% -> 0% of each run, Pallas kernels for 9% -> 14%
where the time goes in v2:
time: 27.8 us; the launch traced here: 27.6 us
  starting transfers between devices  14.8 us (53%)
  Pallas kernels  5.94 us (21%)
  waiting for transfers between devices  5.19 us (19%)
  local copies, waits for them, and re-layouts  0.96 us (3%)
  between operations  0.73 us (3%)
    ppermute x13, starting transfers between devices, exchange(): return lax.ppermute(block, axis, [(i, i ^ step) for i in range(size)])  14.8 us
    ppermute x13, waiting for transfers between devices, exchange(): return lax.ppermute(block, axis, [(i, i ^ step) for i in range(size)])  5.19 us
    pallas_call x1, Pallas kernels, stage(): pl.pallas_call(functools.partial(stage_kernel, len(arrays)), out_shape=[j...  1.54 us
    pallas_call x2, Pallas kernels, begin(): pl.pallas_call(functools.partial(begin_kernel, heads, len(pieces), len(st...  1.21 us
    pallas_call x2, Pallas kernels, output(): pl.pallas_call(functools.partial(output_kernel, steps, len(earlier)), out...  1.2 us
    unnamed x6, local copies, waits for them, and re-layouts  0.96 us
    pallas_call x2, Pallas kernels, finish(): pl.pallas_call(functools.partial(finish_kernel, heads, steps, last, keys)...  0.75 us
    pallas_call x1, Pallas kernels, project(): pl.pallas_call(functools.partial(project_kernel, heads, steps), out_shape...  0.63 us
  transfers between devices with their start and end apart: 13, of which 8 were waited for; matrix products, arithmetic and copies ran while one was open for 0% of the time, Pallas kernels for 14%

profile of v2, /device:TPU:0, one launch (start us, length us, event | category | flops | bytes accessed | tf_op | source)
XLA Modules:
  0.0 27.6 jit_solution(18359066585744454137)
XLA Ops:
  0.0 3.0 %collective-permute-start = (bf16[32,2048]{1,0:T(8,128)(2,1)}, bf16[32,2048]{1,0:T(8,128)(2,1)S(1)}, u32[]{:S(2)}, u32[]{:S(2)}) collective-permute-start(bf16[32,2048]{1,0:T(8,128)(2,1)} %refs_0_.1), channel_id=1, source_target_pairs={{0,2},{1,3},{2,0},{3,1},{4,6},{5,7},{6,4},{7,5},{8,10},{9,11},{10,... | collective-permute-start | bytes 393224 | tf_op jit(solution)/shard_map/ppermute | solution.py:344
  3.0 0.0 collective-permute-start.1
  3.0 0.0 copy-start.1
  3.0 0.9 %copy-done.1 = bf16[32,2048]{1,0:T(8,128)(2,1)S(1)} copy-done((bf16[32,2048]{1,0:T(8,128)(2,1)S(1)}, bf16[32,2048]{1,0:T(8,128)(2,1)}, u32[]{:S(2)}) %copy-start.1) | copy-done | bytes 131096
  3.9 1.5 %stage.1 = (bf16[32,2048]{1,0:T(8,128)(2,1)S(1)}, bf16[64,2048]{1,0:T(8,128)(2,1)S(1)}, bf16[64,2048]{1,0:T(8,128)(2,1)S(1)}, bf16[64,2048]{1,0:T(8,128)(2,1)S(1...) custom-call(bf16[32,2048]{1,0:T(8,128)(2,1)S(1)} %copy-done.1, ...), custom_call_target="tpu_custom_call" | custom-call | flops 436207616 | bytes 1703936 | tf_op jit(solution)/shard_map/stage/pallas_call | solution.py:115
  5.5 1.2 %collective-permute-done.refs_2_ = bf16[32,2048]{1,0:T(8,128)(2,1)S(1)} collective-permute-done((bf16[32,2048]{1,0:T(8,128)(2,1)}, bf16[32,2048]{1,0:T(8,128)(2,1)S(1)}, u32[]{:S(2)}, u32[]{:S(2)}) %collective-permute-start) | collective-permute-done | bytes 131104 | tf_op jit(solution)/shard_map/ppermute | solution.py:344
  6.7 0.0 collective-permute-start.2
  6.7 0.0 collective-permute-done.1.refs_1_
  6.7 0.6 %project.1 = (bf16[96,128]{1,0:T(8,128)(2,1)S(1)}, bf16[96,256]{1,0:T(8,128)(2,1)S(1)}) custom-call(bf16[32,2048]{1,0:T(8,128)(2,1)S(1)} %get-tuple-element.29.refs_0_, bf16[32,2048]{1,0:T(8,128)(2,1)S(1)} %collective-permute-done.1.refs_1_, bf16[32,2048]{1,0:T(8,128)(2,1)S(1)} %collective-permute-done.refs_2_, ...), custom_call_target="tpu_custom_call" | custom-call | flops 150994944 | tf_op jit(solution)/shard_map/project/pallas_call | solution.py:137
  7.3 0.7 %collective-permute-done.2.block_ref = bf16[32,2048]{1,0:T(8,128)(2,1)S(1)} collective-permute-done((bf16[32,2048]{1,0:T(8,128)(2,1)S(1)}, bf16[32,2048]{1,0:T(8,128)(2,1)S(1)}, u32[]{:S(2)}, u32[]{:S(2)}) %collective-permute-start.2) | collective-permute-done | bytes 131104 | tf_op jit(solution)/shard_map/ppermute | solution.py:344
  8.0 0.0 copy-start.2
  8.0 0.4 %keys.1.refs_0_ = bf16[128,256]{1,0:T(8,128)(2,1)S(1)} custom-call(bf16[96,256]{1,0:T(8,128)(2,1)S(1)} %get-tuple-element.40.early_ref, bf16[32,2048]{1,0:T(8,128)(2,1)S(1)} %collective-permute-done.2.block_ref, bf16[64,2048]{1,0:T(8,128)(2,1)S(1)} %get-tuple-element.31.refs_3_.refs_0_, bf16[64,2048]{1,0:T(8,128)(2,1)S(1)} %get-tuple-element.32.refs_4_.refs_1_, ...), custom_call_target="tpu_custom_call" | custom-call | flops 50331648 | tf_op jit(solution)/shard_map/keys/pallas_call | solution.py:165
  8.4 0.0 copy-start
  8.4 2.9 %collective-permute-start.3 = (bf16[128,256]{1,0:T(8,128)(2,1)S(1)}, bf16[128,256]{1,0:T(8,128)(2,1)S(1)}, u32[]{:S(2)}, u32[]{:S(2)}) collective-permute-start(bf16[128,256]{1,0:T(8,128)(2,1)S(1)} %keys.1.refs_0_), channel_id=1, source_target_pairs={{0,16},{4,20},{8,24},{12,28},{16,0},{20,4},{24,8},{28,12},{1,17},{... | collective-permute-start | bytes 196616 | tf_op jit(solution)/shard_map/ppermute | solution.py:344
  11.4 2.5 %collective-permute-start.4 = (bf16[128,256]{1,0:T(8,128)(2,1)S(1)}, bf16[128,256]{1,0:T(8,128)(2,1)S(1)}, u32[]{:S(2)}, u32[]{:S(2)}) collective-permute-start(bf16[128,256]{1,0:T(8,128)(2,1)S(1)} %keys.1.refs_0_), channel_id=1, source_target_pairs={{0,12},{4,8},{8,4},{12,0},{16,28},{20,24},{24,20},{28,16},{1,13},{... | collective-permute-start | bytes 196616 | tf_op jit(solution)/shard_map/ppermute | solution.py:344
  13.9 0.4 %collective-permute-start.5 = (bf16[128,256]{1,0:T(8,128)(2,1)S(1)}, bf16[128,256]{1,0:T(8,128)(2,1)S(1)}, u32[]{:S(2)}, u32[]{:S(2)}) collective-permute-start(bf16[128,256]{1,0:T(8,128)(2,1)S(1)} %keys.1.refs_0_), channel_id=1, source_target_pairs={{0,8},{4,12},{8,0},{12,4},{16,24},{20,28},{24,16},{28,20},{1,9},{5... | collective-permute-start | bytes 196616 | tf_op jit(solution)/shard_map/ppermute | solution.py:344
  14.3 0.5 %collective-permute-start.6 = (bf16[128,256]{1,0:T(8,128)(2,1)S(1)}, bf16[128,256]{1,0:T(8,128)(2,1)S(1)}, u32[]{:S(2)}, u32[]{:S(2)}) collective-permute-start(bf16[128,256]{1,0:T(8,128)(2,1)S(1)} %keys.1.refs_0_), channel_id=1, source_target_pairs={{0,4},{4,0},{8,12},{12,8},{16,20},{20,16},{24,28},{28,24},{1,5},{5... | collective-permute-start | bytes 196616 | tf_op jit(solution)/shard_map/ppermute | solution.py:344
  14.8 0.2 collective-permute-done.3.refs_1_
  15.0 2.4 %collective-permute-start.7 = (bf16[128,256]{1,0:T(8,128)(2,1)S(1)}, bf16[128,256]{1,0:T(8,128)(2,1)S(1)}, u32[]{:S(2)}, u32[]{:S(2)}) collective-permute-start(bf16[128,256]{1,0:T(8,128)(2,1)S(1)} %collective-permute-done.3.refs_1_), channel_id=1, source_target_pairs={{0,12},{4,8},{8,4},{12,0},{16,28},{20,24},{24,20},{28,16},{1,13},{... | collective-permute-start | bytes 196616 | tf_op jit(solution)/shard_map/ppermute | solution.py:344
  17.4 0.6 %collective-permute-start.8 = (bf16[128,256]{1,0:T(8,128)(2,1)S(1)}, bf16[128,256]{1,0:T(8,128)(2,1)S(1)}, u32[]{:S(2)}, u32[]{:S(2)}) collective-permute-start(bf16[128,256]{1,0:T(8,128)(2,1)S(1)} %collective-permute-done.3.refs_1_), channel_id=1, source_target_pairs={{0,8},{4,12},{8,0},{12,4},{16,24},{20,28},{24,16},{28,20},{1,9},{5... | collective-permute-start | bytes 196616 | tf_op jit(solution)/shard_map/ppermute | solution.py:344
  18.0 0.0 collective-permute-done.4.refs_2_
  18.0 0.5 %collective-permute-start.9 = (bf16[128,256]{1,0:T(8,128)(2,1)S(1)}, bf16[128,256]{1,0:T(8,128)(2,1)S(1)}, u32[]{:S(2)}, u32[]{:S(2)}) collective-permute-start(bf16[128,256]{1,0:T(8,128)(2,1)S(1)} %collective-permute-done.3.refs_1_), channel_id=1, source_target_pairs={{0,4},{4,0},{8,12},{12,8},{16,20},{20,16},{24,28},{28,24},{1,5},{5... | collective-permute-start | bytes 196616 | tf_op jit(solution)/shard_map/ppermute | solution.py:344
  19.2 0.3 %queries.1.q_ref = bf16[128,128]{1,0:T(8,128)(2,1)S(1)} custom-call(bf16[96,128]{1,0:T(8,128)(2,1)S(1)} %get-tuple-element.39.early_ref, bf16[32,2048]{1,0:T(8,128)(2,1)S(1)} %collective-permute-done.2.block_ref, bf16[64,2048]{1,0:T(8,128)(2,1)S(1)} %get-tuple-element.31.refs_3_.refs_0_, bf16[64,2048]{1,0:T(8,128)(2,1)S(1)} %get-tuple-element.32.refs_4_.refs_1_, ...), custom_call_target="tpu_custom_call" | custom-call | flops 50331648 | tf_op jit(solution)/shard_map/queries/pallas_call | solution.py:165
  19.5 0.0 collective-permute-done.5.refs_3_
  19.6 0.0 collective-permute-done.6.refs_4_
  19.6 0.7 %begin.1 = (f32[1,256,1]{2,1,0:T(8,128)S(1)}, f32[1,256,1]{2,1,0:T(8,128)S(1)}, f32[1,256,128]{2,1,0:T(8,128)S(1)}) custom-call(bf16[128,128]{1,0:T(8,128)(2,1)S(1)} %queries.1.q_ref, bf16[128,256]{1,0:T(8,128)(2,1)S(1)} %keys.1.refs_0_, bf16[128,256]{1,0:T(8,128)(2,1)S(1)} %collective-permute-done.3.refs_1_, ...), custom_call_target="tpu_custom_call" | custom-call | flops 83886080 | tf_op jit(solution)/shard_map/begin/pallas_call | solution.py:285
  20.3 0.3 %collective-permute-done.7.refs_3_ = bf16[128,256]{1,0:T(8,128)(2,1)S(1)} collective-permute-done((bf16[128,256]{1,0:T(8,128)(2,1)S(1)}, bf16[128,256]{1,0:T(8,128)(2,1)S(1)}, u32[]{:S(2)}, u32[]{:S(2)}) %collective-permute-start.7) | collective-permute-done | bytes 65568 | tf_op jit(solution)/shard_map/ppermute | solution.py:344
  20.6 1.0 %collective-permute-done.8.refs_4_ = bf16[128,256]{1,0:T(8,128)(2,1)S(1)} collective-permute-done((bf16[128,256]{1,0:T(8,128)(2,1)S(1)}, bf16[128,256]{1,0:T(8,128)(2,1)S(1)}, u32[]{:S(2)}, u32[]{:S(2)}) %collective-permute-start.8) | collective-permute-done | bytes 65568 | tf_op jit(solution)/shard_map/ppermute | solution.py:344
  21.6 0.5 %middle.1 = (f32[1,256,1]{2,1,0:T(8,128)S(1)}, f32[1,256,1]{2,1,0:T(8,128)S(1)}, f32[1,256,128]{2,1,0:T(8,128)S(1)}) custom-call(bf16[128,128]{1,0:T(8,128)(2,1)S(1)} %queries.1.q_ref, f32[1,256,1]{2,1,0:T(8,128)S(1)} %get-tuple-element.41.refs_0_, f32[1,256,1]{2,1,0:T(8,128)S(1)} %get-tuple-element.42.refs_1_, ...), custom_call_target="tpu_custom_call" | custom-call | flops 33554432 | tf_op jit(solution)/shard_map/middle/pallas_call | solution.py:285
  22.2 0.1 collective-permute-done.9.refs_3_
  22.3 0.0 copy-done.2
  22.3 0.6 %attend.1 = (bf16[32,128]{1,0:T(8,128)(2,1)S(1)}, bf16[32,128]{1,0:T(8,128)(2,1)S(1)}, bf16[32,128]{1,0:T(8,128)(2,1)S(1)}, bf16[32,128]{1,0:T(8,128)(2,1)S(1)}) custom-call(bf16[128,128]{1,0:T(8,128)(2,1)S(1)} %queries.1.q_ref, f32[1,256,1]{2,1,0:T(8,128)S(1)} %get-tuple-element.44.refs_0_, f32[1,256,1]{2,1,0:T(8,128)S(1)} %get-tuple-element.45.refs_1_, ...), custom_call_target="tpu_custom_call" | custom-call | flops 16777216 | tf_op jit(solution)/shard_map/attend/pallas_call | solution.py:300
  22.9 0.1 collective-permute-start.10
  23.0 1.6 %collective-permute-start.11 = (bf16[32,128]{1,0:T(8,128)(2,1)S(1)}, bf16[32,128]{1,0:T(8,128)(2,1)S(1)}, u32[]{:S(2)}, u32[]{:S(2)}) collective-permute-start(bf16[32,128]{1,0:T(8,128)(2,1)S(1)} %get-tuple-element.49), channel_id=1, source_target_pairs={{0,2},{1,3},{2,0},{3,1},{4,6},{5,7},{6,4},{7,5},{8,10},{9,11},{10,... | collective-permute-start | bytes 24584 | tf_op jit(solution)/shard_map/ppermute | solution.py:344
  24.5 0.3 %collective-permute-start.12 = (bf16[32,128]{1,0:T(8,128)(2,1)S(1)}, bf16[32,128]{1,0:T(8,128)(2,1)S(1)}, u32[]{:S(2)}, u32[]{:S(2)}) collective-permute-start(bf16[32,128]{1,0:T(8,128)(2,1)S(1)} %get-tuple-element.50), channel_id=1, source_target_pairs={{0,1},{1,0},{2,3},{3,2},{4,5},{5,4},{6,7},{7,6},{8,9},{9,8},{10,11... | collective-permute-start | bytes 24584 | tf_op jit(solution)/shard_map/ppermute | solution.py:344
  24.8 1.3 %collective-permute-done.10.refs_1_ = bf16[32,128]{1,0:T(8,128)(2,1)S(1)} collective-permute-done((bf16[32,128]{1,0:T(8,128)(2,1)S(1)}, bf16[32,128]{1,0:T(8,128)(2,1)S(1)}, u32[]{:S(2)}, u32[]{:S(2)}) %collective-permute-start.10) | collective-permute-done | bytes 8224 | tf_op jit(solution)/shard_map/ppermute | solution.py:344
  26.1 0.0 copy-done
  26.1 0.3 early.1.refs_0_
  26.4 0.3 %collective-permute-done.11.refs_1_ = bf16[32,128]{1,0:T(8,128)(2,1)S(1)} collective-permute-done((bf16[32,128]{1,0:T(8,128)(2,1)S(1)}, bf16[32,128]{1,0:T(8,128)(2,1)S(1)}, u32[]{:S(2)}, u32[]{:S(2)}) %collective-permute-start.11) | collective-permute-done | bytes 8224 | tf_op jit(solution)/shard_map/ppermute | solution.py:344
  26.7 0.0 collective-permute-done.12.refs_2_
  26.7 0.9 %output.1 = bf16[32,2048]{1,0:T(8,128)(2,1)} custom-call(f32[32,2048]{1,0:T(8,128)S(1)} %early.1.refs_0_, bf16[32,128]{1,0:T(8,128)(2,1)S(1)} %collective-permute-done.11.refs_1_, bf16[32,128]{1,0:T(8,128)(2,1)S(1)} %collective-permute-done.12.refs_2_, bf16[512,2048]{1,0:T(8,128)(2,1)S(1)} %copy-done), custom_call_target="tpu_custom_call" | custom-call | flops 33554432 | tf_op jit(solution)/shard_map/output/pallas_call | solution.py:329
Async XLA Ops:
  0.0 6.7 %collective-permute-start = (bf16[32,2048]{1,0:T(8,128)(2,1)}, bf16[32,2048]{1,0:T(8,128)(2,1)S(1)}, u32[]{:S(2)}, u32[]{:S(2)}) collective-permute-start(bf16[32,2048]{1,0:T(8,128)(2,1)} %refs_0_.1), channel_id=1, source_target_pairs={{0,2},{1,3},{2,0},{3,1},{4,6},{5,7},{6,4},{7,5},{8,10},{9,11},{10,... | collective-permute-start | bytes 393224 | tf_op jit(solution)/shard_map/ppermute | solution.py:344
  3.0 3.7 %collective-permute-start.1 = (bf16[32,2048]{1,0:T(8,128)(2,1)}, bf16[32,2048]{1,0:T(8,128)(2,1)S(1)}, u32[]{:S(2)}, u32[]{:S(2)}) collective-permute-start(bf16[32,2048]{1,0:T(8,128)(2,1)} %refs_0_.1), channel_id=1, source_target_pairs={{0,1},{1,0},{2,3},{3,2},{4,5},{5,4},{6,7},{7,6},{8,9},{9,8},{10,11... | collective-permute-start | bytes 393224 | tf_op jit(solution)/shard_map/ppermute | solution.py:344
  3.0 0.9 %copy-start.1 = (bf16[32,2048]{1,0:T(8,128)(2,1)S(1)}, bf16[32,2048]{1,0:T(8,128)(2,1)}, u32[]{:S(2)}) copy-start(bf16[32,2048]{1,0:T(8,128)(2,1)} %refs_0_.1) | copy-start | bytes 393220
  6.7 1.3 %collective-permute-start.2 = (bf16[32,2048]{1,0:T(8,128)(2,1)S(1)}, bf16[32,2048]{1,0:T(8,128)(2,1)S(1)}, u32[]{:S(2)}, u32[]{:S(2)}) collective-permute-start(bf16[32,2048]{1,0:T(8,128)(2,1)S(1)} %collective-permute-done.refs_2_), channel_id=1, source_target_pairs={{0,1},{1,0},{2,3},{3,2},{4,5},{5,4},{6,7},{7,6},{8,9},{9,8},{10,11... | collective-permute-start | bytes 393224 | tf_op jit(solution)/shard_map/ppermute | solution.py:344
  8.0 14.3 %copy-start.2 = (f32[128]{0:T(128)S(1)}, f32[128]{0:T(128)}, u32[]{:S(2)}) copy-start(f32[128]{0:T(128)} %param.17) | copy-start | bytes 1540
  8.4 17.7 %copy-start = (bf16[512,2048]{1,0:T(8,128)(2,1)S(1)}, bf16[512,2048]{1,0:T(8,128)(2,1)}, u32[]{:S(2)}) copy-start(bf16[512,2048]{1,0:T(8,128)(2,1)} %refs_3_.1) | copy-start | bytes 6291460
  8.4 6.6 %collective-permute-start.3 = (bf16[128,256]{1,0:T(8,128)(2,1)S(1)}, bf16[128,256]{1,0:T(8,128)(2,1)S(1)}, u32[]{:S(2)}, u32[]{:S(2)}) collective-permute-start(bf16[128,256]{1,0:T(8,128)(2,1)S(1)} %keys.1.refs_0_), channel_id=1, source_target_pairs={{0,16},{4,20},{8,24},{12,28},{16,0},{20,4},{24,8},{28,12},{1,17},{... | collective-permute-start | bytes 196616 | tf_op jit(solution)/shard_map/ppermute | solution.py:344
  11.4 6.7 %collective-permute-start.4 = (bf16[128,256]{1,0:T(8,128)(2,1)S(1)}, bf16[128,256]{1,0:T(8,128)(2,1)S(1)}, u32[]{:S(2)}, u32[]{:S(2)}) collective-permute-start(bf16[128,256]{1,0:T(8,128)(2,1)S(1)} %keys.1.refs_0_), channel_id=1, source_target_pairs={{0,12},{4,8},{8,4},{12,0},{16,28},{20,24},{24,20},{28,16},{1,13},{... | collective-permute-start | bytes 196616 | tf_op jit(solution)/shard_map/ppermute | solution.py:344
  13.9 5.7 %collective-permute-start.5 = (bf16[128,256]{1,0:T(8,128)(2,1)S(1)}, bf16[128,256]{1,0:T(8,128)(2,1)S(1)}, u32[]{:S(2)}, u32[]{:S(2)}) collective-permute-start(bf16[128,256]{1,0:T(8,128)(2,1)S(1)} %keys.1.refs_0_), channel_id=1, source_target_pairs={{0,8},{4,12},{8,0},{12,4},{16,24},{20,28},{24,16},{28,20},{1,9},{5... | collective-permute-start | bytes 196616 | tf_op jit(solution)/shard_map/ppermute | solution.py:344
  14.3 5.2 %collective-permute-start.6 = (bf16[128,256]{1,0:T(8,128)(2,1)S(1)}, bf16[128,256]{1,0:T(8,128)(2,1)S(1)}, u32[]{:S(2)}, u32[]{:S(2)}) collective-permute-start(bf16[128,256]{1,0:T(8,128)(2,1)S(1)} %keys.1.refs_0_), channel_id=1, source_target_pairs={{0,4},{4,0},{8,12},{12,8},{16,20},{20,16},{24,28},{28,24},{1,5},{5... | collective-permute-start | bytes 196616 | tf_op jit(solution)/shard_map/ppermute | solution.py:344
  15.0 5.6 %collective-permute-start.7 = (bf16[128,256]{1,0:T(8,128)(2,1)S(1)}, bf16[128,256]{1,0:T(8,128)(2,1)S(1)}, u32[]{:S(2)}, u32[]{:S(2)}) collective-permute-start(bf16[128,256]{1,0:T(8,128)(2,1)S(1)} %collective-permute-done.3.refs_1_), channel_id=1, source_target_pairs={{0,12},{4,8},{8,4},{12,0},{16,28},{20,24},{24,20},{28,16},{1,13},{... | collective-permute-start | bytes 196616 | tf_op jit(solution)/shard_map/ppermute | solution.py:344
  17.4 4.3 %collective-permute-start.8 = (bf16[128,256]{1,0:T(8,128)(2,1)S(1)}, bf16[128,256]{1,0:T(8,128)(2,1)S(1)}, u32[]{:S(2)}, u32[]{:S(2)}) collective-permute-start(bf16[128,256]{1,0:T(8,128)(2,1)S(1)} %collective-permute-done.3.refs_1_), channel_id=1, source_target_pairs={{0,8},{4,12},{8,0},{12,4},{16,24},{20,28},{24,16},{28,20},{1,9},{5... | collective-permute-start | bytes 196616 | tf_op jit(solution)/shard_map/ppermute | solution.py:344
  18.0 4.3 %collective-permute-start.9 = (bf16[128,256]{1,0:T(8,128)(2,1)S(1)}, bf16[128,256]{1,0:T(8,128)(2,1)S(1)}, u32[]{:S(2)}, u32[]{:S(2)}) collective-permute-start(bf16[128,256]{1,0:T(8,128)(2,1)S(1)} %collective-permute-done.3.refs_1_), channel_id=1, source_target_pairs={{0,4},{4,0},{8,12},{12,8},{16,20},{20,16},{24,28},{28,24},{1,5},{5... | collective-permute-start | bytes 196616 | tf_op jit(solution)/shard_map/ppermute | solution.py:344
  22.9 3.2 %collective-permute-start.10 = (bf16[32,128]{1,0:T(8,128)(2,1)S(1)}, bf16[32,128]{1,0:T(8,128)(2,1)S(1)}, u32[]{:S(2)}, u32[]{:S(2)}) collective-permute-start(bf16[32,128]{1,0:T(8,128)(2,1)S(1)} %get-tuple-element.48), channel_id=1, source_target_pairs={{0,3},{1,2},{2,1},{3,0},{4,7},{5,6},{6,5},{7,4},{8,11},{9,10},{10,... | collective-permute-start | bytes 24584 | tf_op jit(solution)/shard_map/ppermute | solution.py:344
  23.0 3.7 %collective-permute-start.11 = (bf16[32,128]{1,0:T(8,128)(2,1)S(1)}, bf16[32,128]{1,0:T(8,128)(2,1)S(1)}, u32[]{:S(2)}, u32[]{:S(2)}) collective-permute-start(bf16[32,128]{1,0:T(8,128)(2,1)S(1)} %get-tuple-element.49), channel_id=1, source_target_pairs={{0,2},{1,3},{2,0},{3,1},{4,6},{5,7},{6,4},{7,5},{8,10},{9,11},{10,... | collective-permute-start | bytes 24584 | tf_op jit(solution)/shard_map/ppermute | solution.py:344
  24.5 2.2 %collective-permute-start.12 = (bf16[32,128]{1,0:T(8,128)(2,1)S(1)}, bf16[32,128]{1,0:T(8,128)(2,1)S(1)}, u32[]{:S(2)}, u32[]{:S(2)}) collective-permute-start(bf16[32,128]{1,0:T(8,128)(2,1)S(1)} %get-tuple-element.50), channel_id=1, source_target_pairs={{0,1},{1,0},{2,3},{3,2},{4,5},{5,4},{6,7},{7,6},{8,9},{9,8},{10,11... | collective-permute-start | bytes 24584 | tf_op jit(solution)/shard_map/ppermute | solution.py:344

commit v3 on v2

--- a/solution.py
+++ b/solution.py
@@ -143,32 +143,34 @@
     )(*blocks, *weights)
 
 
-def finish_kernel(heads, steps, last, keys, early_ref, block_ref, *refs):
+def finish_kernel(heads, steps, late_steps, keys, early_ref, *refs):
+    blocks, refs = refs[: len(late_steps)], refs[len(late_steps) :]
     weight_refs, out_ref = refs[:8], refs[8]
-    count = block_ref.shape[0]
+    count = blocks[0].shape[0]
     for at, step in enumerate(steps):
         out_ref[pl.ds(place_of(step, count), count), :] = early_ref[at * count : (at + 1) * count, :]
-    place = place_of(last, count)
-    project_blocks(
-        [block_ref],
-        [place],
-        weight_refs,
-        heads,
-        None if keys else out_ref,
-        out_ref if keys else None,
-        pl.ds(place, count),
-    )
-
-
-def finish(early, steps, block, last, weights, heads, groups, keys):
-    count, depth = block.shape
-    return pl.pallas_call(
-        functools.partial(finish_kernel, heads, steps, last, keys),
+    for step, block in zip(late_steps, blocks):
+        place = place_of(step, count)
+        project_blocks(
+            [block],
+            [place],
+            weight_refs,
+            heads,
+            None if keys else out_ref,
+            out_ref if keys else None,
+            pl.ds(place, count),
+        )
+
+
+def finish(early, steps, blocks, late_steps, weights, heads, groups, keys):
+    count, depth = blocks[0].shape
+    return pl.pallas_call(
+        functools.partial(finish_kernel, heads, steps, late_steps, keys),
         out_shape=jax.ShapeDtypeStruct((count * groups, early.shape[1]), early.dtype),
-        cost_estimate=project_cost(count, depth, heads),
+        cost_estimate=project_cost(count * len(blocks), depth, heads),
         compiler_params=pltpu.CompilerParams(vmem_limit_bytes=8 * MIB),
         name="keys" if keys else "queries",
-    )(early, block, *weights)
+    )(early, *blocks, *weights)
 
 
 def both_of(pair):
@@ -241,13 +243,13 @@
             ref[head] = value
 
 
-def attend_kernel(heads, pieces, held, groups, steps, q_ref, *refs):
+def attend_kernel(heads, pieces, held, groups, q_ref, *refs):
     state_refs, refs = refs[:held], refs[held:]
     kv_refs, (mixing_ref, gain_ref), out_refs = refs[:pieces], refs[pieces : pieces + 2], refs[pieces + 2 :]
     total_rows = q_ref.shape[0]
     share = total_rows // groups
-    rows = share * len(steps)
-    places = [place_of(step, share) for step in steps]
+    rows = total_rows
+    places = [place_of(step, share) for step in range(groups)]
     for head in range(heads):
         columns = slice(head * PAIR, (head + 1) * PAIR)
         pair = jnp.concatenate([q_ref[pl.ds(at, share), columns] for at in places], axis=0)
@@ -293,14 +295,14 @@
     )(queries, *state, *pieces)
 
 
-def attend(queries, state, pieces, mixing, gain, heads, groups, steps):
+def attend(queries, state, pieces, mixing, gain, heads, groups):
     rows = queries.shape[0]
     keys = sum(p.shape[0] for p in pieces)
     share = jax.ShapeDtypeStruct((rows // groups, heads * PAIR), jnp.bfloat16)
     return pl.pallas_call(
-        functools.partial(attend_kernel, heads, len(pieces), len(state), groups, steps),
-        out_shape=[share] * len(steps),
-        cost_estimate=attend_cost(rows * len(steps) // groups, keys, heads),
+        functools.partial(attend_kernel, heads, len(pieces), len(state), groups),
+        out_shape=[share] * groups,
+        cost_estimate=attend_cost(rows, keys, heads),
         compiler_params=pltpu.CompilerParams(vmem_limit_bytes=attend_grant(rows, keys, heads)),
         name="attend",
     )(queries, *state, *pieces, mixing.reshape(1, heads), gain.reshape(1, PAIR))
@@ -363,24 +365,29 @@
     row_count = own_rows * groups
     heads = query_one.shape[1] // HEAD
     weights = (query_one.T, query_two.T, key_one.T, key_two.T, value_weight)
-    across = exchange(tokens, "tp", 2)
-    beside = exchange(tokens, "tp", 1)
+    half = groups // 2
+    near = tuple(range(1, half))
+    across = exchange(tokens, "tp", half)
+    beside = [exchange(tokens, "tp", step) for step in near]
     own, *held = stage([tokens, *weights], own_rows * groups)
     across, own = lax.optimization_barrier((across, own))
-    last = exchange(across, "tp", 1)
-    early = project([own, beside, across], (0, 1, 2), held, heads)
-    packed = finish(early[1], (0, 1, 2), last, 3, held, heads, groups, True)
-    queries = finish(early[0], (0, 1, 2), last, 3, held, heads, groups, False)
+    late = [exchange(across, "tp", step) for step in near]
+    early_steps, late_steps = (0, *near, half), tuple(half + step for step in near)
+    early = project([own, *beside, across], early_steps, held, heads)
+    packed = finish(early[1], early_steps, late, late_steps, held, heads, groups, True)
+    queries = finish(early[0], early_steps, late, late_steps, held, heads, groups, False)
     first, second = gather_pieces(packed, "sp")
     state = begin(queries, [], first, heads) if first else []
     if len(second) > 1:
-        state, second = begin(queries, state, second[:-1], heads), second[-1:]
+        state, second = begin(queries, state, second[:1], heads), second[1:]
     rest = (mixing, head_gain, heads, groups)
-    own, beside, across, aside = attend(queries, state, second, *rest, (0, 1, 2, 3))
-    across, aside = exchange(across, "tp", 2), exchange(aside, "tp", 3)
-    beside = exchange(beside, "tp", 1)
-    early = output([], [own, aside], (0, 3), out_weight, jnp.float32)
-    return output([early], [across, beside], (2, 1), out_weight, jnp.bfloat16)
+    shares = attend(queries, state, second, *rest)
+    last = groups - 1
+    others = tuple(range(last - 1, 0, -1))
+    farthest = exchange(shares[last], "tp", last)
+    shares = [farthest] + [exchange(shares[step], "tp", step) for step in others] + [shares[0]]
+    early = output([], [shares[-1], farthest], (0, last), out_weight, jnp.float32)
+    return output([early], shares[1:-1], others, out_weight, jnp.bfloat16)
 
 
 def solution(mesh):

time: 27.8 us -> 27.9 us (level)
  no operation moved by 1% of the time
where the time goes in v3:
time: 27.9 us; the launch traced here: 27.7 us
  starting transfers between devices  14.8 us (53%)
  Pallas kernels  5.93 us (21%)
  waiting for transfers between devices  5.26 us (19%)
  local copies, waits for them, and re-layouts  0.96 us (3%)
  between operations  0.73 us (3%)
    ppermute x13, starting transfers between devices, exchange(): return lax.ppermute(block, axis, [(i, i ^ step) for i in range(size)])  14.8 us
    ppermute x13, waiting for transfers between devices, exchange(): return lax.ppermute(block, axis, [(i, i ^ step) for i in range(size)])  5.26 us
    pallas_call x1, Pallas kernels, stage(): pl.pallas_call(functools.partial(stage_kernel, len(arrays)), out_shape=[j...  1.54 us
    pallas_call x2, Pallas kernels, output(): pl.pallas_call(functools.partial(output_kernel, steps, len(earlier)), out...  1.2 us
    pallas_call x2, Pallas kernels, begin(): pl.pallas_call(functools.partial(begin_kernel, heads, len(pieces), len(st...  1.15 us
    unnamed x6, local copies, waits for them, and re-layouts  0.96 us
    pallas_call x2, Pallas kernels, finish(): pl.pallas_call(functools.partial(finish_kernel, heads, steps, late_steps,...  0.75 us
    pallas_call x1, Pallas kernels, attend(): pl.pallas_call(functools.partial(attend_kernel, heads, len(pieces), len(s...  0.67 us
  transfers between devices with their start and end apart: 13, of which 8 were waited for; matrix products, arithmetic and copies ran while one was open for 0% of the time, Pallas kernels for 14%

profile of v3, /device:TPU:0, one launch (start us, length us, event | category | flops | bytes accessed | tf_op | source)
XLA Modules:
  0.0 27.7 jit_solution(10039296356177530293)
XLA Ops:
  0.0 3.0 %collective-permute-start = (bf16[32,2048]{1,0:T(8,128)(2,1)}, bf16[32,2048]{1,0:T(8,128)(2,1)S(1)}, u32[]{:S(2)}, u32[]{:S(2)}) collective-permute-start(bf16[32,2048]{1,0:T(8,128)(2,1)} %refs_0_.1), channel_id=1, source_target_pairs={{0,2},{1,3},{2,0},{3,1},{4,6},{5,7},{6,4},{7,5},{8,10},{9,11},{10,... | collective-permute-start | bytes 393224 | tf_op jit(solution)/shard_map/ppermute | solution.py:346
  3.0 0.0 collective-permute-start.1
  3.0 0.0 copy-start.1
  3.0 0.9 %copy-done.1 = bf16[32,2048]{1,0:T(8,128)(2,1)S(1)} copy-done((bf16[32,2048]{1,0:T(8,128)(2,1)S(1)}, bf16[32,2048]{1,0:T(8,128)(2,1)}, u32[]{:S(2)}) %copy-start.1) | copy-done | bytes 131096
  3.9 1.5 %stage.1 = (bf16[32,2048]{1,0:T(8,128)(2,1)S(1)}, bf16[64,2048]{1,0:T(8,128)(2,1)S(1)}, bf16[64,2048]{1,0:T(8,128)(2,1)S(1)}, bf16[64,2048]{1,0:T(8,128)(2,1)S(1...) custom-call(bf16[32,2048]{1,0:T(8,128)(2,1)S(1)} %copy-done.1, ...), custom_call_target="tpu_custom_call" | custom-call | flops 436207616 | bytes 1703936 | tf_op jit(solution)/shard_map/stage/pallas_call | solution.py:115
  5.5 1.2 %collective-permute-done.refs_2_ = bf16[32,2048]{1,0:T(8,128)(2,1)S(1)} collective-permute-done((bf16[32,2048]{1,0:T(8,128)(2,1)}, bf16[32,2048]{1,0:T(8,128)(2,1)S(1)}, u32[]{:S(2)}, u32[]{:S(2)}) %collective-permute-start) | collective-permute-done | bytes 131104 | tf_op jit(solution)/shard_map/ppermute | solution.py:346
  6.7 0.0 collective-permute-start.2
  6.7 0.0 collective-permute-done.1.refs_1_
  6.7 0.6 %project.1 = (bf16[96,128]{1,0:T(8,128)(2,1)S(1)}, bf16[96,256]{1,0:T(8,128)(2,1)S(1)}) custom-call(bf16[32,2048]{1,0:T(8,128)(2,1)S(1)} %get-tuple-element.29.refs_0_, bf16[32,2048]{1,0:T(8,128)(2,1)S(1)} %collective-permute-done.1.refs_1_, bf16[32,2048]{1,0:T(8,128)(2,1)S(1)} %collective-permute-done.refs_2_, ...), custom_call_target="tpu_custom_call" | custom-call | flops 150994944 | tf_op jit(solution)/shard_map/project/pallas_call | solution.py:137
  7.3 0.7 %collective-permute-done.2.refs_0_ = bf16[32,2048]{1,0:T(8,128)(2,1)S(1)} collective-permute-done((bf16[32,2048]{1,0:T(8,128)(2,1)S(1)}, bf16[32,2048]{1,0:T(8,128)(2,1)S(1)}, u32[]{:S(2)}, u32[]{:S(2)}) %collective-permute-start.2) | collective-permute-done | bytes 131104 | tf_op jit(solution)/shard_map/ppermute | solution.py:346
  8.0 0.0 copy-start.2
  8.0 0.4 %keys.1.refs_0_ = bf16[128,256]{1,0:T(8,128)(2,1)S(1)} custom-call(bf16[96,256]{1,0:T(8,128)(2,1)S(1)} %get-tuple-element.40.early_ref, bf16[32,2048]{1,0:T(8,128)(2,1)S(1)} %collective-permute-done.2.refs_0_, bf16[64,2048]{1,0:T(8,128)(2,1)S(1)} %get-tuple-element.31.refs_3_.refs_1_, bf16[64,2048]{1,0:T(8,128)(2,1)S(1)} %get-tuple-element.32.refs_4_.refs_2_, ...), custom_call_target="tpu_custom_call" | custom-call | flops 50331648 | tf_op jit(solution)/shard_map/keys/pallas_call | solution.py:167
  8.4 0.0 copy-start
  8.4 2.9 %collective-permute-start.3 = (bf16[128,256]{1,0:T(8,128)(2,1)S(1)}, bf16[128,256]{1,0:T(8,128)(2,1)S(1)}, u32[]{:S(2)}, u32[]{:S(2)}) collective-permute-start(bf16[128,256]{1,0:T(8,128)(2,1)S(1)} %keys.1.refs_0_), channel_id=1, source_target_pairs={{0,16},{4,20},{8,24},{12,28},{16,0},{20,4},{24,8},{28,12},{1,17},{... | collective-permute-start | bytes 196616 | tf_op jit(solution)/shard_map/ppermute | solution.py:346
  11.4 2.5 %collective-permute-start.4 = (bf16[128,256]{1,0:T(8,128)(2,1)S(1)}, bf16[128,256]{1,0:T(8,128)(2,1)S(1)}, u32[]{:S(2)}, u32[]{:S(2)}) collective-permute-start(bf16[128,256]{1,0:T(8,128)(2,1)S(1)} %keys.1.refs_0_), channel_id=1, source_target_pairs={{0,12},{4,8},{8,4},{12,0},{16,28},{20,24},{24,20},{28,16},{1,13},{... | collective-permute-start | bytes 196616 | tf_op jit(solution)/shard_map/ppermute | solution.py:346
  13.9 0.4 %collective-permute-start.5 = (bf16[128,256]{1,0:T(8,128)(2,1)S(1)}, bf16[128,256]{1,0:T(8,128)(2,1)S(1)}, u32[]{:S(2)}, u32[]{:S(2)}) collective-permute-start(bf16[128,256]{1,0:T(8,128)(2,1)S(1)} %keys.1.refs_0_), channel_id=1, source_target_pairs={{0,8},{4,12},{8,0},{12,4},{16,24},{20,28},{24,16},{28,20},{1,9},{5... | collective-permute-start | bytes 196616 | tf_op jit(solution)/shard_map/ppermute | solution.py:346
  14.3 0.5 %collective-permute-start.6 = (bf16[128,256]{1,0:T(8,128)(2,1)S(1)}, bf16[128,256]{1,0:T(8,128)(2,1)S(1)}, u32[]{:S(2)}, u32[]{:S(2)}) collective-permute-start(bf16[128,256]{1,0:T(8,128)(2,1)S(1)} %keys.1.refs_0_), channel_id=1, source_target_pairs={{0,4},{4,0},{8,12},{12,8},{16,20},{20,16},{24,28},{28,24},{1,5},{5... | collective-permute-start | bytes 196616 | tf_op jit(solution)/shard_map/ppermute | solution.py:346
  14.8 0.2 collective-permute-done.3.refs_1_
  15.0 2.4 %collective-permute-start.7 = (bf16[128,256]{1,0:T(8,128)(2,1)S(1)}, bf16[128,256]{1,0:T(8,128)(2,1)S(1)}, u32[]{:S(2)}, u32[]{:S(2)}) collective-permute-start(bf16[128,256]{1,0:T(8,128)(2,1)S(1)} %collective-permute-done.3.refs_1_), channel_id=1, source_target_pairs={{0,12},{4,8},{8,4},{12,0},{16,28},{20,24},{24,20},{28,16},{1,13},{... | collective-permute-start | bytes 196616 | tf_op jit(solution)/shard_map/ppermute | solution.py:346
  17.4 0.6 %collective-permute-start.8 = (bf16[128,256]{1,0:T(8,128)(2,1)S(1)}, bf16[128,256]{1,0:T(8,128)(2,1)S(1)}, u32[]{:S(2)}, u32[]{:S(2)}) collective-permute-start(bf16[128,256]{1,0:T(8,128)(2,1)S(1)} %collective-permute-done.3.refs_1_), channel_id=1, source_target_pairs={{0,8},{4,12},{8,0},{12,4},{16,24},{20,28},{24,16},{28,20},{1,9},{5... | collective-permute-start | bytes 196616 | tf_op jit(solution)/shard_map/ppermute | solution.py:346
  18.0 0.0 collective-permute-done.4.refs_2_
  18.0 0.5 %collective-permute-start.9 = (bf16[128,256]{1,0:T(8,128)(2,1)S(1)}, bf16[128,256]{1,0:T(8,128)(2,1)S(1)}, u32[]{:S(2)}, u32[]{:S(2)}) collective-permute-start(bf16[128,256]{1,0:T(8,128)(2,1)S(1)} %collective-permute-done.3.refs_1_), channel_id=1, source_target_pairs={{0,4},{4,0},{8,12},{12,8},{16,20},{20,16},{24,28},{28,24},{1,5},{5... | collective-permute-start | bytes 196616 | tf_op jit(solution)/shard_map/ppermute | solution.py:346
  19.2 0.3 %queries.1.q_ref = bf16[128,128]{1,0:T(8,128)(2,1)S(1)} custom-call(bf16[96,128]{1,0:T(8,128)(2,1)S(1)} %get-tuple-element.39.early_ref, bf16[32,2048]{1,0:T(8,128)(2,1)S(1)} %collective-permute-done.2.refs_0_, bf16[64,2048]{1,0:T(8,128)(2,1)S(1)} %get-tuple-element.31.refs_3_.refs_1_, bf16[64,2048]{1,0:T(8,128)(2,1)S(1)} %get-tuple-element.32.refs_4_.refs_2_, ...), custom_call_target="tpu_custom_call" | custom-call | flops 50331648 | tf_op jit(solution)/shard_map/queries/pallas_call | solution.py:167
  19.5 0.0 collective-permute-done.5.refs_3_
  19.6 0.0 collective-permute-done.6.refs_4_
  19.6 0.7 %begin.1 = (f32[1,256,1]{2,1,0:T(8,128)S(1)}, f32[1,256,1]{2,1,0:T(8,128)S(1)}, f32[1,256,128]{2,1,0:T(8,128)S(1)}) custom-call(bf16[128,128]{1,0:T(8,128)(2,1)S(1)} %queries.1.q_ref, bf16[128,256]{1,0:T(8,128)(2,1)S(1)} %keys.1.refs_0_, bf16[128,256]{1,0:T(8,128)(2,1)S(1)} %collective-permute-done.3.refs_1_, ...), custom_call_target="tpu_custom_call" | custom-call | flops 83886080 | tf_op jit(solution)/shard_map/begin/pallas_call | solution.py:287
  20.3 0.3 %collective-permute-done.7.refs_3_ = bf16[128,256]{1,0:T(8,128)(2,1)S(1)} collective-permute-done((bf16[128,256]{1,0:T(8,128)(2,1)S(1)}, bf16[128,256]{1,0:T(8,128)(2,1)S(1)}, u32[]{:S(2)}, u32[]{:S(2)}) %collective-permute-start.7) | collective-permute-done | bytes 65568 | tf_op jit(solution)/shard_map/ppermute | solution.py:346
  20.6 0.5 %middle.1 = (f32[1,256,1]{2,1,0:T(8,128)S(1)}, f32[1,256,1]{2,1,0:T(8,128)S(1)}, f32[1,256,128]{2,1,0:T(8,128)S(1)}) custom-call(bf16[128,128]{1,0:T(8,128)(2,1)S(1)} %queries.1.q_ref, f32[1,256,1]{2,1,0:T(8,128)S(1)} %get-tuple-element.41.refs_0_, f32[1,256,1]{2,1,0:T(8,128)S(1)} %get-tuple-element.42.refs_1_, ...), custom_call_target="tpu_custom_call" | custom-call | flops 16777216 | tf_op jit(solution)/shard_map/middle/pallas_call | solution.py:287
  21.1 0.6 %collective-permute-done.8.refs_3_ = bf16[128,256]{1,0:T(8,128)(2,1)S(1)} collective-permute-done((bf16[128,256]{1,0:T(8,128)(2,1)S(1)}, bf16[128,256]{1,0:T(8,128)(2,1)S(1)}, u32[]{:S(2)}, u32[]{:S(2)}) %collective-permute-start.8) | collective-permute-done | bytes 65568 | tf_op jit(solution)/shard_map/ppermute | solution.py:346
  21.6 0.6 %collective-permute-done.9.refs_4_ = bf16[128,256]{1,0:T(8,128)(2,1)S(1)} collective-permute-done((bf16[128,256]{1,0:T(8,128)(2,1)S(1)}, bf16[128,256]{1,0:T(8,128)(2,1)S(1)}, u32[]{:S(2)}, u32[]{:S(2)}) %collective-permute-start.9) | collective-permute-done | bytes 65568 | tf_op jit(solution)/shard_map/ppermute | solution.py:346
  22.3 0.0 copy-done.2
  22.3 0.7 %attend.1 = (bf16[32,128]{1,0:T(8,128)(2,1)S(1)}, bf16[32,128]{1,0:T(8,128)(2,1)S(1)}, bf16[32,128]{1,0:T(8,128)(2,1)S(1)}, bf16[32,128]{1,0:T(8,128)(2,1)S(1)}) custom-call(bf16[128,128]{1,0:T(8,128)(2,1)S(1)} %queries.1.q_ref, f32[1,256,1]{2,1,0:T(8,128)S(1)} %get-tuple-element.44.refs_0_, f32[1,256,1]{2,1,0:T(8,128)S(1)} %get-tuple-element.45.refs_1_, ...), custom_call_target="tpu_custom_call" | custom-call | flops 33554432 | tf_op jit(solution)/shard_map/attend/pallas_call | solution.py:302
  23.0 0.1 collective-permute-start.10
  23.0 1.6 %collective-permute-start.11 = (bf16[32,128]{1,0:T(8,128)(2,1)S(1)}, bf16[32,128]{1,0:T(8,128)(2,1)S(1)}, u32[]{:S(2)}, u32[]{:S(2)}) collective-permute-start(bf16[32,128]{1,0:T(8,128)(2,1)S(1)} %get-tuple-element.49), channel_id=1, source_target_pairs={{0,2},{1,3},{2,0},{3,1},{4,6},{5,7},{6,4},{7,5},{8,10},{9,11},{10,... | collective-permute-start | bytes 24584 | tf_op jit(solution)/shard_map/ppermute | solution.py:346
  24.6 0.3 %collective-permute-start.12 = (bf16[32,128]{1,0:T(8,128)(2,1)S(1)}, bf16[32,128]{1,0:T(8,128)(2,1)S(1)}, u32[]{:S(2)}, u32[]{:S(2)}) collective-permute-start(bf16[32,128]{1,0:T(8,128)(2,1)S(1)} %get-tuple-element.50), channel_id=1, source_target_pairs={{0,1},{1,0},{2,3},{3,2},{4,5},{5,4},{6,7},{7,6},{8,9},{9,8},{10,11... | collective-permute-start | bytes 24584 | tf_op jit(solution)/shard_map/ppermute | solution.py:346
  24.9 1.3 %collective-permute-done.10.refs_1_ = bf16[32,128]{1,0:T(8,128)(2,1)S(1)} collective-permute-done((bf16[32,128]{1,0:T(8,128)(2,1)S(1)}, bf16[32,128]{1,0:T(8,128)(2,1)S(1)}, u32[]{:S(2)}, u32[]{:S(2)}) %collective-permute-start.10) | collective-permute-done | bytes 8224 | tf_op jit(solution)/shard_map/ppermute | solution.py:346
  26.1 0.0 copy-done
  26.1 0.3 early.1.refs_0_
  26.4 0.3 %collective-permute-done.11.refs_1_ = bf16[32,128]{1,0:T(8,128)(2,1)S(1)} collective-permute-done((bf16[32,128]{1,0:T(8,128)(2,1)S(1)}, bf16[32,128]{1,0:T(8,128)(2,1)S(1)}, u32[]{:S(2)}, u32[]{:S(2)}) %collective-permute-start.11) | collective-permute-done | bytes 8224 | tf_op jit(solution)/shard_map/ppermute | solution.py:346
  26.8 0.0 collective-permute-done.12.refs_2_
  26.8 0.9 %output.1 = bf16[32,2048]{1,0:T(8,128)(2,1)} custom-call(f32[32,2048]{1,0:T(8,128)S(1)} %early.1.refs_0_, bf16[32,128]{1,0:T(8,128)(2,1)S(1)} %collective-permute-done.11.refs_1_, bf16[32,128]{1,0:T(8,128)(2,1)S(1)} %collective-permute-done.12.refs_2_, bf16[512,2048]{1,0:T(8,128)(2,1)S(1)} %copy-done), custom_call_target="tpu_custom_call" | custom-call | flops 33554432 | tf_op jit(solution)/shard_map/output/pallas_call | solution.py:331
Async XLA Ops:
  0.0 6.7 %collective-permute-start = (bf16[32,2048]{1,0:T(8,128)(2,1)}, bf16[32,2048]{1,0:T(8,128)(2,1)S(1)}, u32[]{:S(2)}, u32[]{:S(2)}) collective-permute-start(bf16[32,2048]{1,0:T(8,128)(2,1)} %refs_0_.1), channel_id=1, source_target_pairs={{0,2},{1,3},{2,0},{3,1},{4,6},{5,7},{6,4},{7,5},{8,10},{9,11},{10,... | collective-permute-start | bytes 393224 | tf_op jit(solution)/shard_map/ppermute | solution.py:346
  3.0 3.7 %collective-permute-start.1 = (bf16[32,2048]{1,0:T(8,128)(2,1)}, bf16[32,2048]{1,0:T(8,128)(2,1)S(1)}, u32[]{:S(2)}, u32[]{:S(2)}) collective-permute-start(bf16[32,2048]{1,0:T(8,128)(2,1)} %refs_0_.1), channel_id=1, source_target_pairs={{0,1},{1,0},{2,3},{3,2},{4,5},{5,4},{6,7},{7,6},{8,9},{9,8},{10,11... | collective-permute-start | bytes 393224 | tf_op jit(solution)/shard_map/ppermute | solution.py:346
  3.0 0.9 %copy-start.1 = (bf16[32,2048]{1,0:T(8,128)(2,1)S(1)}, bf16[32,2048]{1,0:T(8,128)(2,1)}, u32[]{:S(2)}) copy-start(bf16[32,2048]{1,0:T(8,128)(2,1)} %refs_0_.1) | copy-start | bytes 393220
  6.7 1.3 %collective-permute-start.2 = (bf16[32,2048]{1,0:T(8,128)(2,1)S(1)}, bf16[32,2048]{1,0:T(8,128)(2,1)S(1)}, u32[]{:S(2)}, u32[]{:S(2)}) collective-permute-start(bf16[32,2048]{1,0:T(8,128)(2,1)S(1)} %collective-permute-done.refs_2_), channel_id=1, source_target_pairs={{0,1},{1,0},{2,3},{3,2},{4,5},{5,4},{6,7},{7,6},{8,9},{9,8},{10,11... | collective-permute-start | bytes 393224 | tf_op jit(solution)/shard_map/ppermute | solution.py:346
  8.0 14.3 %copy-start.2 = (f32[128]{0:T(128)S(1)}, f32[128]{0:T(128)}, u32[]{:S(2)}) copy-start(f32[128]{0:T(128)} %param.17) | copy-start | bytes 1540
  8.4 17.7 %copy-start = (bf16[512,2048]{1,0:T(8,128)(2,1)S(1)}, bf16[512,2048]{1,0:T(8,128)(2,1)}, u32[]{:S(2)}) copy-start(bf16[512,2048]{1,0:T(8,128)(2,1)} %refs_3_.1) | copy-start | bytes 6291460
  8.4 6.6 %collective-permute-start.3 = (bf16[128,256]{1,0:T(8,128)(2,1)S(1)}, bf16[128,256]{1,0:T(8,128)(2,1)S(1)}, u32[]{:S(2)}, u32[]{:S(2)}) collective-permute-start(bf16[128,256]{1,0:T(8,128)(2,1)S(1)} %keys.1.refs_0_), channel_id=1, source_target_pairs={{0,16},{4,20},{8,24},{12,28},{16,0},{20,4},{24,8},{28,12},{1,17},{... | collective-permute-start | bytes 196616 | tf_op jit(solution)/shard_map/ppermute | solution.py:346
  11.4 6.7 %collective-permute-start.4 = (bf16[128,256]{1,0:T(8,128)(2,1)S(1)}, bf16[128,256]{1,0:T(8,128)(2,1)S(1)}, u32[]{:S(2)}, u32[]{:S(2)}) collective-permute-start(bf16[128,256]{1,0:T(8,128)(2,1)S(1)} %keys.1.refs_0_), channel_id=1, source_target_pairs={{0,12},{4,8},{8,4},{12,0},{16,28},{20,24},{24,20},{28,16},{1,13},{... | collective-permute-start | bytes 196616 | tf_op jit(solution)/shard_map/ppermute | solution.py:346
  13.9 5.7 %collective-permute-start.5 = (bf16[128,256]{1,0:T(8,128)(2,1)S(1)}, bf16[128,256]{1,0:T(8,128)(2,1)S(1)}, u32[]{:S(2)}, u32[]{:S(2)}) collective-permute-start(bf16[128,256]{1,0:T(8,128)(2,1)S(1)} %keys.1.refs_0_), channel_id=1, source_target_pairs={{0,8},{4,12},{8,0},{12,4},{16,24},{20,28},{24,16},{28,20},{1,9},{5... | collective-permute-start | bytes 196616 | tf_op jit(solution)/shard_map/ppermute | solution.py:346
  14.3 5.2 %collective-permute-start.6 = (bf16[128,256]{1,0:T(8,128)(2,1)S(1)}, bf16[128,256]{1,0:T(8,128)(2,1)S(1)}, u32[]{:S(2)}, u32[]{:S(2)}) collective-permute-start(bf16[128,256]{1,0:T(8,128)(2,1)S(1)} %keys.1.refs_0_), channel_id=1, source_target_pairs={{0,4},{4,0},{8,12},{12,8},{16,20},{20,16},{24,28},{28,24},{1,5},{5... | collective-permute-start | bytes 196616 | tf_op jit(solution)/shard_map/ppermute | solution.py:346
  15.0 5.6 %collective-permute-start.7 = (bf16[128,256]{1,0:T(8,128)(2,1)S(1)}, bf16[128,256]{1,0:T(8,128)(2,1)S(1)}, u32[]{:S(2)}, u32[]{:S(2)}) collective-permute-start(bf16[128,256]{1,0:T(8,128)(2,1)S(1)} %collective-permute-done.3.refs_1_), channel_id=1, source_target_pairs={{0,12},{4,8},{8,4},{12,0},{16,28},{20,24},{24,20},{28,16},{1,13},{... | collective-permute-start | bytes 196616 | tf_op jit(solution)/shard_map/ppermute | solution.py:346
  17.4 4.3 %collective-permute-start.8 = (bf16[128,256]{1,0:T(8,128)(2,1)S(1)}, bf16[128,256]{1,0:T(8,128)(2,1)S(1)}, u32[]{:S(2)}, u32[]{:S(2)}) collective-permute-start(bf16[128,256]{1,0:T(8,128)(2,1)S(1)} %collective-permute-done.3.refs_1_), channel_id=1, source_target_pairs={{0,8},{4,12},{8,0},{12,4},{16,24},{20,28},{24,16},{28,20},{1,9},{5... | collective-permute-start | bytes 196616 | tf_op jit(solution)/shard_map/ppermute | solution.py:346
  18.0 4.3 %collective-permute-start.9 = (bf16[128,256]{1,0:T(8,128)(2,1)S(1)}, bf16[128,256]{1,0:T(8,128)(2,1)S(1)}, u32[]{:S(2)}, u32[]{:S(2)}) collective-permute-start(bf16[128,256]{1,0:T(8,128)(2,1)S(1)} %collective-permute-done.3.refs_1_), channel_id=1, source_target_pairs={{0,4},{4,0},{8,12},{12,8},{16,20},{20,16},{24,28},{28,24},{1,5},{5... | collective-permute-start | bytes 196616 | tf_op jit(solution)/shard_map/ppermute | solution.py:346
  23.0 3.2 %collective-permute-start.10 = (bf16[32,128]{1,0:T(8,128)(2,1)S(1)}, bf16[32,128]{1,0:T(8,128)(2,1)S(1)}, u32[]{:S(2)}, u32[]{:S(2)}) collective-permute-start(bf16[32,128]{1,0:T(8,128)(2,1)S(1)} %get-tuple-element.48), channel_id=1, source_target_pairs={{0,3},{1,2},{2,1},{3,0},{4,7},{5,6},{6,5},{7,4},{8,11},{9,10},{10,... | collective-permute-start | bytes 24584 | tf_op jit(solution)/shard_map/ppermute | solution.py:346
  23.0 3.7 %collective-permute-start.11 = (bf16[32,128]{1,0:T(8,128)(2,1)S(1)}, bf16[32,128]{1,0:T(8,128)(2,1)S(1)}, u32[]{:S(2)}, u32[]{:S(2)}) collective-permute-start(bf16[32,128]{1,0:T(8,128)(2,1)S(1)} %get-tuple-element.49), channel_id=1, source_target_pairs={{0,2},{1,3},{2,0},{3,1},{4,6},{5,7},{6,4},{7,5},{8,10},{9,11},{10,... | collective-permute-start | bytes 24584 | tf_op jit(solution)/shard_map/ppermute | solution.py:346
  24.6 2.2 %collective-permute-start.12 = (bf16[32,128]{1,0:T(8,128)(2,1)S(1)}, bf16[32,128]{1,0:T(8,128)(2,1)S(1)}, u32[]{:S(2)}, u32[]{:S(2)}) collective-permute-start(bf16[32,128]{1,0:T(8,128)(2,1)S(1)} %get-tuple-element.50), channel_id=1, source_target_pairs={{0,1},{1,0},{2,3},{3,2},{4,5},{5,4},{6,7},{7,6},{8,9},{9,8},{10,11... | collective-permute-start | bytes 24584 | tf_op jit(solution)/shard_map/ppermute | solution.py:346
